TPU v7x, 256 devices: a whole 4x4x8 slice. The times are simulated.
256 devices in a mesh: sp: 64 (over z, x, core), tp: 4 (over y).
Axes of the slice: x: 4, y: 4, z: 8, core: 2. Of those that a mesh axis runs over, the one named last changes fastest.
Arguments:
- stream: bfloat16 [32768, 2048], P(('sp', 'tp')), may hold values from -6 to 6
- queries: bfloat16 [32768, 512], P('sp', 'tp'), may hold values from -6 to 6
- key_rows: bfloat16 [32768, 512], P('sp', 'tp'), may hold values from -6 to 6
- values: bfloat16 [32768, 1024], P('sp', 'tp'), may hold values from -6 to 6
- out_gate: bfloat16 [32768, 1024], P('sp', 'tp'), may hold values from -6 to 6
- fwd_decay: float32 [32768, 512], P('sp', 'tp'), may hold values from -14 to 14
- bwd_decay: float32 [32768, 512], P('sp', 'tp'), may hold values from -14 to 14
- head_gain: float32 [1024], P('tp'), may hold values from 0.1 to 1.9
- out_proj: bfloat16 [1024, 2048], replicated, may hold values from -0.1875 to 0.1875
- mix_gain: float32 [2048], replicated, may hold values from 0.1 to 1.9
- ffn_gain: float32 [2048], replicated, may hold values from 0.1 to 1.9
- moe_gain: float32 [2048], replicated, may hold values from 0.1 to 1.9
- routes: int32 [32768, 2], P(('sp', 'tp')), may hold values from 0 to 63, all different within a row; in each aligned block of 128 rows (0 to 127, 128 to 255, ...) at most 6 rows name the same one
- route_weight: float32 [32768, 2], P(('sp', 'tp')), may hold values from 0.25 to 2.5
- expert_gate: bfloat16 [64, 2048, 1024], P('sp', None, 'tp'), may hold values from -0.125 to 0.125
- expert_up: bfloat16 [64, 2048, 1024], P('sp', None, 'tp'), may hold values from -0.125 to 0.125
- expert_down: bfloat16 [64, 1024, 2048], P('sp', 'tp'), may hold values from -0.1875 to 0.1875
- shared_gate: bfloat16 [2048, 512], P(None, 'tp'), may hold values from -0.125 to 0.125
- shared_up: bfloat16 [2048, 512], P(None, 'tp'), may hold values from -0.125 to 0.125
- shared_down: bfloat16 [512, 2048], P('tp'), may hold values from -0.25 to 0.25
Outputs:
- updated: bfloat16 [32768, 2048], P(('sp', 'tp'))
Inputs may be any that keep to these rules, and one draw needn't show every extreme that they name: `routes`: each row names 2 different experts. Among the rows of one device no expert is named more than 6 times, and in every draw some device names some expert exactly 6 times.
All inputs are finite; a program needn't handle non-finite values.
Results may differ from a plain program's by a relative error of at most 0.023.
Values may be sent and summed in bfloat16 or wider, within the bound.
A program may use at most 128 MiB of HBM per device.

v0:
```python
import jax
import jax.numpy as jnp
from jax import lax
from jax.sharding import Mesh
from jax.sharding import PartitionSpec as P

KEY_CHANNELS = 64
DV = 128
BLK = 64
TOPK = 2
SP = ("sp_0", "sp_1", "sp_2")
SP_TP = ("sp_0", "sp_1", "sp_2", "tp")


EPS = 1e-06
GATE_NORM = 16.0
ROPE_BASE = 10000.0


def gathered_once(array, axis):
    leaves = jax.tree.leaves(array)
    sequence = sorted(range(len(leaves)), key=lambda k: -leaves[k].size)
    width = (1, *leaves[sequence[0]].shape)[-1]
    lines = [
        jnp.pad(leaves[k].reshape(-1), (0, -leaves[k].size % width)).reshape(-1, width)
        for k in sequence
    ]
    both, at, found = (lax.all_gather(jnp.concatenate(lines), axis), 0, {})
    for k, line in zip(sequence, lines):
        share = both[:, at : at + len(line)].reshape(len(both), -1)
        found[k] = share[:, : leaves[k].size].reshape(-1, *leaves[k].shape)
        at += len(line)
    numbers = iter(range(len(leaves)))
    return jax.tree.map(lambda _: found[next(numbers)], array)


def prefix(array, axis, combine, identity):
    length, position = (lax.axis_size(axis), lax.axis_index(axis))
    everything = gathered_once(
        jax.tree.map(
            lambda part, kind: part.astype(kind),
            array,
            jax.tree.map(lambda a: jnp.bfloat16 if a.dtype == jnp.float32 else a.dtype, array),
        ),
        axis,
    )
    start = jax.tree.map(
        lambda part, zero: jnp.broadcast_to(jnp.asarray(zero, part.dtype), part.shape),
        array,
        identity,
    )

    def step(k, before):
        reached = k < position
        new = combine(
            before, jax.tree.map(lambda part, own: part[k].astype(own.dtype), everything, array)
        )
        return jax.tree.map(lambda a, b: jnp.where(reached, a, b), new, before)

    return lax.fori_loop(0, length, step, start)


def neutral_like(array, identity):
    return jax.tree.map(
        lambda a, e: jnp.broadcast_to(jnp.asarray(e, a.dtype), a.shape), array, identity
    )


def entering(array, axes, combine, identity):
    before = start = neutral_like(array, identity)
    so_far = array
    for axis in reversed(axes):
        length, position = (lax.axis_size(axis), lax.axis_index(axis))
        pieces = gathered_once(
            jax.tree.map(
                lambda part, kind: part.astype(kind),
                so_far,
                jax.tree.map(lambda a: jnp.bfloat16 if a.dtype == jnp.float32 else a.dtype, array),
            ),
            axis,
        )
        inside, so_far = (start, start)
        for k in reversed(range(length)):
            passed = k > position
            so_far = combine(
                so_far, jax.tree.map(lambda part, own: part[k].astype(own.dtype), pieces, array)
            )
            inside = jax.tree.map(lambda new, old: jnp.where(passed, new, old), so_far, inside)
        before = combine(inside, before)
    return before


def normalize(tensor):
    return tensor * lax.rsqrt(jnp.mean(tensor * tensor, axis=-1, keepdims=True) + EPS)


def rotate(tensor, positions):
    half_width = tensor.shape[-1] // 2
    frequency = ROPE_BASE ** (-jnp.arange(half_width, dtype=jnp.float32) / half_width)
    angles = positions[:, None] * frequency[None, :]
    cosine = jnp.cos(angles)[:, None, :]
    sine_part = jnp.sin(angles)[:, None, :]
    front_half = tensor[..., :half_width]
    back_half = tensor[..., half_width:]
    return jnp.concatenate(
        [front_half * cosine - back_half * sine_part, front_half * sine_part + back_half * cosine],
        axis=-1,
    )


def blockwise(query_rows, key_data, value_matrix, log_decay, start_state):
    length, head_count, key_width = query_rows.shape
    value_width = value_matrix.shape[-1]
    block_count = length // BLK
    query_blocks = query_rows.reshape(block_count, BLK, head_count, key_width)
    key_blocks = key_data.reshape(block_count, BLK, head_count, key_width)
    value_blocks = value_matrix.reshape(block_count, BLK, head_count, value_width)
    cumul = jnp.cumsum(log_decay.reshape(block_count, BLK, head_count, key_width), axis=1)
    middle = cumul[:, BLK // 2 - 1 : BLK // 2]
    query_scaled = query_blocks * jnp.exp(cumul - middle)
    key_scaled = key_blocks * jnp.exp(middle - cumul)
    scores = jnp.einsum("nthk,nshk->nhts", query_scaled, key_scaled)
    lower_mask = jnp.arange(BLK)[:, None] >= jnp.arange(BLK)[None, :]
    scores = jnp.where(lower_mask, scores, 0.0)
    within = jnp.einsum("nhts,nshv->nthv", scores, value_blocks)
    last_cumul = cumul[:, -1:]
    query_in = query_blocks * jnp.exp(cumul)
    key_out = key_blocks * jnp.exp(last_cumul - cumul)
    block_decay = jnp.exp(last_cumul[:, 0])

    def advance(carried_state, pieces):
        query_segment, key_segment, value_segment, decay_segment = pieces
        across_blocks = jnp.einsum("asu,sun->asn", query_segment, carried_state)
        carried_state = carried_state * decay_segment[:, :, None] + jnp.einsum(
            "jco,jcm->com", key_segment, value_segment
        )
        return (carried_state, across_blocks)

    final_state, across_blocks = lax.scan(
        advance, start_state, (query_in, key_out, value_blocks, block_decay)
    )
    return ((within + across_blocks).reshape(length, head_count, value_width), final_state)


def readout(query_rows, log_decay, carried_state):
    cumul = jnp.cumsum(log_decay, axis=0)
    return jnp.einsum("asu,sun->asn", query_rows * jnp.exp(cumul), carried_state)


def compose(earlier, later):
    return (earlier[0] * later[0], earlier[1] * later[0][:, :, None] + later[1])


def feed_forward(row_data, gate_mat, up_mat, down_mat):
    hidden = (
        jax.nn.silu(jnp.dot(row_data, gate_mat, preferred_element_type=jnp.float32))
        * jnp.dot(row_data, up_mat, preferred_element_type=jnp.float32)
    ).astype(jnp.bfloat16)
    return jnp.dot(hidden, down_mat, preferred_element_type=jnp.float32)


def place_slots(route_block, experts):
    flat_ids = route_block.reshape(-1)
    onehot = (flat_ids[:, None] == jnp.arange(experts, dtype=jnp.int32)[None, :]).astype(jnp.int32)
    before = jnp.cumsum(onehot, axis=0) - onehot
    return (flat_ids, jnp.sum(before * onehot, axis=1))


def fill_slots(row_data, route_block, experts, capacity):
    flat_ids, slot_ids = place_slots(route_block, experts)
    token_ids = jnp.arange(flat_ids.shape[0], dtype=jnp.int32) // route_block.shape[1]
    buffer = jnp.zeros((experts, capacity, row_data.shape[1]), row_data.dtype)
    return buffer.at[flat_ids, slot_ids].set(row_data[token_ids])


def body(
    stream,
    queries,
    key_rows,
    values,
    out_gate,
    fwd_decay,
    bwd_decay,
    head_gain,
    out_proj,
    mix_gain,
    ffn_gain,
    moe_gain,
    routes,
    route_weight,
    expert_gate,
    expert_up,
    expert_down,
    shared_gate,
    shared_up,
    shared_down,
):
    tokens_here = stream.shape[0]
    span_rows = queries.shape[0]
    heads_here = queries.shape[1] // KEY_CHANNELS
    offset = lax.axis_index(SP) * span_rows
    positions = (offset + jnp.arange(span_rows, dtype=jnp.int32)).astype(jnp.float32)
    query_rows = rotate(
        queries.astype(jnp.float32).reshape(span_rows, heads_here, KEY_CHANNELS)
        * KEY_CHANNELS ** (-0.5),
        positions,
    )
    key_data = rotate(
        key_rows.astype(jnp.float32).reshape(span_rows, heads_here, KEY_CHANNELS), positions
    )
    value_matrix = values.astype(jnp.float32).reshape(span_rows, heads_here, DV)
    fwd_log = jax.nn.log_sigmoid(fwd_decay).reshape(span_rows, heads_here, KEY_CHANNELS) / GATE_NORM
    bwd_log = (
        jax.nn.log_sigmoid(bwd_decay[::-1]).reshape(span_rows, heads_here, KEY_CHANNELS) / GATE_NORM
    )
    query_back = query_rows[::-1]
    key_back = key_data[::-1]
    value_back = value_matrix[::-1]
    zero_state = jnp.zeros((heads_here, KEY_CHANNELS, DV), jnp.float32)
    identity = (jnp.ones((heads_here, KEY_CHANNELS), jnp.float32), zero_state)
    fwd_out, fwd_final = blockwise(query_rows, key_data, value_matrix, fwd_log, zero_state)
    bwd_out, bwd_final = blockwise(query_back, key_back, value_back, bwd_log, zero_state)
    fwd_summary = (jnp.exp(jnp.sum(fwd_log, axis=0)), fwd_final)
    bwd_summary = (jnp.exp(jnp.sum(bwd_log, axis=0)), bwd_final)
    fwd_carry = prefix(fwd_summary, SP, compose, identity)[1]
    bwd_carry = entering(bwd_summary, SP, compose, identity)[1]
    fwd_out = fwd_out + readout(query_rows, fwd_log, fwd_carry)
    bwd_out = bwd_out + readout(query_back, bwd_log, bwd_carry)
    combined = normalize(fwd_out + bwd_out[::-1]) * head_gain.reshape(heads_here, DV)
    head_mixed = (
        combined.reshape(span_rows, -1) * jax.nn.silu(out_gate.astype(jnp.float32))
    ).astype(jnp.bfloat16)
    mixed_out = lax.all_to_all(head_mixed, "tp", split_axis=0, concat_axis=1, tiled=True)
    projected = jnp.dot(mixed_out, out_proj, preferred_element_type=jnp.float32)
    residual = (stream.astype(jnp.float32) + normalize(projected) * mix_gain).astype(jnp.bfloat16)
    normed = (normalize(residual.astype(jnp.float32)) * ffn_gain).astype(jnp.bfloat16)
    experts = lax.axis_size(SP)
    groups = lax.axis_size("tp")
    capacity = max(2, 3 * tokens_here * TOPK // (2 * experts))
    model_width = normed.shape[1]
    arrived = lax.all_to_all(
        fill_slots(normed, routes, experts, capacity), SP, split_axis=0, concat_axis=0, tiled=True
    )
    fanned, shared_flat = (
        lax.all_gather(arrived.reshape(experts * capacity, model_width), "tp", axis=0, tiled=True),
        lax.all_gather(normed, "tp", axis=0, tiled=True),
    )
    routed_rows = fanned.reshape(groups, experts * capacity, model_width)
    shared_rows = shared_flat.reshape(groups, tokens_here, model_width)
    width_rows = experts * capacity + tokens_here
    number = width_rows * lax.axis_size("tp") // width_rows
    routed_part = routed_rows.reshape(number * experts * capacity, model_width)
    shared_part = shared_rows.reshape(number * tokens_here, model_width)
    routed_out = feed_forward(routed_part, expert_gate[0], expert_up[0], expert_down[0]).reshape(
        number, experts * capacity, model_width
    )
    shared_out = feed_forward(shared_part, shared_gate, shared_up, shared_down).reshape(
        number, tokens_here, model_width
    )
    summed = lax.psum_scatter(
        jnp.concatenate([routed_out, shared_out], axis=1)
        .reshape(width_rows * lax.axis_size("tp"), model_width)
        .astype(jnp.bfloat16),
        "tp",
        scatter_dimension=0,
        tiled=True,
    ).astype(jnp.float32)
    routed_done = (
        summed[: experts * capacity].astype(jnp.bfloat16).reshape(experts, capacity, model_width)
    )
    routed_back = lax.all_to_all(routed_done, SP, split_axis=0, concat_axis=0, tiled=True)
    shared_sum = summed[experts * capacity :]
    flat_ids, slot_ids = place_slots(routes, experts)
    picked = routed_back.reshape(experts * capacity, model_width)[flat_ids * capacity + slot_ids]
    picked = picked.astype(jnp.float32).reshape(tokens_here, TOPK, model_width)
    mixture = shared_sum + jnp.sum(picked * route_weight[:, :, None], axis=1)
    return (residual.astype(jnp.float32) + normalize(mixture) * moe_gain).astype(jnp.bfloat16)


def solution(mesh):
    finer = Mesh(mesh.devices.reshape(8, 4, 2, mesh.shape["tp"]), ("sp_0", "sp_1", "sp_2", "tp"))
    placed = (
        P(SP_TP, None),
        P(SP, "tp"),
        P(SP, "tp"),
        P(SP, "tp"),
        P(SP, "tp"),
        P(SP, "tp"),
        P(SP, "tp"),
        P("tp"),
        P(),
        P(),
        P(),
        P(),
        P(SP_TP, None),
        P(SP_TP, None),
        P(SP, None, "tp"),
        P(SP, None, "tp"),
        P(SP, "tp", None),
        P(None, "tp"),
        P(None, "tp"),
        P("tp", None),
    )
    return jax.shard_map(
        body, mesh=finer, in_specs=placed, out_specs=P(SP_TP, None), check_vma=False
    )
```

profile of v0, /device:TPU:1, one launch (start us, length us, event | category | flops | bytes accessed | tf_op | source)
XLA Modules:
  0.0 552.5 jit_solution(17728160664577737282)
XLA Ops:
  10.0 13.0 %fusion.178 = f32[8,64,2,64]{3,0,1,2:T(8,128)S(1)} fusion(f32[8,64,2,64]{3,0,1,2:T(8,128)S(1)} %copy.134), kind=kOutput, calls=%fused_computation.308 | output fusion | flops 4128768 | bytes 524288 | tf_op jit(solution)/shard_map/jit(cumsum)/reduce_window_sum | solution.py:118
  29.1 1.8 copy.142
  30.9 2.1 reshape.855
  33.0 2.0 copy.147
  36.9 24.3 %while.40 = (s32[]{:T(128)}, f32[2,64,128]{2,1,0:T(8,128)S(1)}, f32[8,64,2,128]{3,1,2,0:T(8,128)}, f32[8,2,64]{2,0,1:T(8,128)S(1)}, f32[8,64,2,64]{3,0,1,2:T(8,1...) while((s32[]{:T(128)}, f32[2,64,128]{2,1,0:T(8,128)S(1)}, ...), condition=%wide.region_2.3_spmd.clone, body=%wide.region_1.2_spmd.clone.sunk | while | flops 4259843 | bytes 494192 | solution.py:139
  61.9 1.7 reshape_reshape.8
  63.6 3.1 rev.15
  66.7 3.1 rev.17
  70.8 2.0 copy.156
  76.3 1.9 reshape.758
  83.2 24.4 %while.42 = (s32[]{:T(128)}, f32[2,64,128]{2,1,0:T(8,128)S(1)}, f32[8,64,2,128]{3,1,2,0:T(8,128)}, f32[8,2,64]{2,0,1:T(8,128)S(1)}, f32[8,64,2,64]{3,0,1,2:T(8,1...) while((s32[]{:T(128)}, f32[2,64,128]{2,1,0:T(8,128)S(1)}, ...), condition=%wide.region_10.11_spmd.clone, body=%wide.region_9.10_spmd.clone.sunk | while | flops 4259843 | bytes 494192 | solution.py:139
  83.2 1.3 constant_dynamic-slice_fusion.12
  107.7 2.4 fusion.24
  110.6 1.9 copy.149
  112.5 2.0 copy.154
  114.6 4.7 all-gather.5
  119.4 10.0 %all-gather.6 = bf16[4,129,128]{2,1,0:T(8,128)(2,1)S(1)} all-gather(bf16[1,129,128]{2,1,0:T(8,128)(2,1)S(1)} %maximum_bitcast_fusion.2), channel_id=4, replica_groups=mesh['sp_0'=8,'sp_1'=4,'sp_2'=2,'tp'=4] {'sp_1'}, dimensions={0}, use_global_device_ids=true | all-gather | bytes 165120 | tf_op jit(solution)/shard_map/all_gather | solution.py:28
  130.1 21.1 %all-gather.7 = bf16[8,129,128]{2,1,0:T(8,128)(2,1)S(1)} all-gather(bf16[1,129,128]{2,1,0:T(8,128)(2,1)S(1)} %maximum_bitcast_fusion.3), channel_id=5, replica_groups=mesh['sp_0'=8,'sp_1'=4,'sp_2'=2,'tp'=4] {'sp_0'}, dimensions={0}, use_global_device_ids=true | all-gather | bytes 297216 | tf_op jit(solution)/shard_map/all_gather | solution.py:28
  153.6 1.6 fusion.20
  155.5 2.4 reduce-window.24
  160.3 3.0 rev.19
  163.3 2.4 reduce-window.20
  168.1 1.6 slice-done.1
  169.7 8.8 %while.41 = (s32[]{:T(128)}, f32[2,64,128]{2,1,0:T(8,128)S(1)}, s32[]{:T(128)}, bf16[64,2,64]{2,1,0:T(2,128)(2,1)S(1)}, bf16[64,2,64,128]{3,2,1,0:T(8,128)(2,1)S(1)}, /*index=5*/s32[]{:T(128)}, s32[]{:T(128)}) while((s32[]{:T(128)}, f32[2,64,128]{2,1,0:T(8,128)S(1)}, s32[]{:T(128)}, bf16[64,2,64]{2,1,0:T(2,128)(2,1)S(1)}, ...), condition=%wide.region_5.6_spmd.clone, body=%wide.region_4.5_spmd.clone.sunk | while | flops 82052 | bytes 165225 | solution.py:60
  178.5 1.8 multiply_reduce_fusion.3
  181.5 4.3 all-to-all-start
  185.8 5.5 all-to-all-done
  191.5 3.1 multiply_reduce_fusion.2
  197.8 2.3 gather_fusion
  200.3 33.6 %scatter_fusion = bf16[64,6,2048]{2,0,1:T(8,128)(2,1)S(1)} fusion(bf16[64,6,2048]{2,0,1:T(8,128)(2,1)S(1)} %broadcast_in_dim.40, s32[256]{0:T(256)S(1)} %bitcast.315, bf16[256,2048]{1,0:T(8,128)(2,1)} %gather_fusion), kind=kCustom, calls=%fused_computation.2 | custom fusion | bytes 3147776 | tf_op jit(solution)/shard_map/scatter | solution.py:173
  234.9 66.7 %all_to_all.29 = bf16[64,6,2048]{2,1,0:T(8,128)(2,1)S(1)} all-to-all(bf16[64,6,2048]{2,1,0:T(8,128)(2,1)S(1)} %copy.181), channel_id=1, replica_groups=mesh['sp_0'=8,'sp_1'=4,'sp_2'=2,'tp'=4] {'sp_0','sp_1','sp_2'}, dimensions={0} | all-to-all | bytes 3145728 | tf_op jit(solution)/shard_map/all_to_all | solution.py:241
  301.6 1.5 reshape.768
  303.2 2.5 fusion.180
  305.7 4.9 convolution_convert_fusion.1
  310.6 56.5 %all-gather.12.cloned.1.call-done = bf16[1536,2048]{1,0:T(8,128)(2,1)} async-done(((bf16[384,2048]{1,0:T(8,128)(2,1)}), bf16[1536,2048]{1,0:T(8,128)(2,1)}) %all-gather.12.cloned.1.call-update) | async-done | bytes 6291472 | tf_op jit(solution)/shard_map/all_gather | solution.py:245
  367.0 5.1 fusion.32
  372.1 2.1 fusion.17
  374.2 4.5 convolution_convert_fusion
  378.7 7.6 %pad_maximum_fusion = bf16[4,512,2048]{2,1,0:T(8,128)(2,1)} fusion(bf16[4,128,2048]{2,1,0:T(8,128)(2,1)S(1)} %bitcast.316, bf16[4,384,2048]{2,1,0:T(8,128)(2,1)} %convolution_convert_fusion), kind=kLoop, calls=%fused_computation.32 | loop fusion | flops 16777216 | bytes 16777216 | tf_op jit(solution)/shard_map/concatenate | solution.py:261
  386.4 84.0 %reduce-scatter.2.cloned.1.call-done = bf16[512,2048]{1,0:T(8,128)(2,1)} async-done(((bf16[2048,2048]{1,0:T(8,128)(2,1)}), bf16[512,2048]{1,0:T(8,128)(2,1)}) %reduce-scatter.2.cloned.1.call-update) | async-done | bytes 2097168 | tf_op jit(solution)/shard_map/reduce_scatter | solution.py:260
  470.4 1.4 slice-done
  471.8 1.6 reshape.770
  473.4 11.1 %all-to-all-start.2 = ((bf16[64,6,2048]{2,1,0:T(8,128)(2,1)}), bf16[64,6,2048]{2,1,0:T(8,128)(2,1)}, u32[]{:S(2)}, u32[]{:S(2)}) async-start(bf16[64,6,2048]{2,1,0:T(8,128)(2,1)} %reshape.770), calls=%async_computation.3 | async-start | bytes 4194304 | tf_op jit(solution)/shard_map/all_to_all | solution.py:271
  484.6 49.5 %all-to-all-done.2 = bf16[64,6,2048]{2,1,0:T(8,128)(2,1)} async-done(((bf16[64,6,2048]{2,1,0:T(8,128)(2,1)}), bf16[64,6,2048]{2,1,0:T(8,128)(2,1)}, u32[]{:S(2)}, u32[]{:S(2)}) %all-to-all-start.2) | async-done | bytes 1572896 | tf_op jit(solution)/shard_map/all_to_all | solution.py:271
  534.0 2.6 reshape.771
  536.6 2.3 gather_fusion.1
  539.0 2.4 reshape.813
  541.4 3.2 multiply_reduce_fusion
  (385 shorter events, 90.5 us)
Async XLA Ops:
  6.5 367.7 %copy-start = (bf16[1,256,2048]{2,1,0:T(8,128)(2,1)S(1)}, bf16[1,256,2048]{2,1,0:T(8,128)(2,1)}, u32[]{:S(2)}) copy-start(bf16[1,256,2048]{2,1,0:T(8,128)(2,1)} %param.42) | copy-start | bytes 3145732
  6.5 160.5 %all-gather.16.cloned.1.call-start = ((), (), s32[]{:S(2)}) async-start(), calls=%async_computation.7 | async-start | bytes 2263040 | tf_op jit(solution)/shard_map/all_gather | solution.py:28
  9.2 13.9 %copy-start.21 = (bf16[512,128]{1,0:T(8,128)(2,1)S(1)}, bf16[512,128]{1,0:T(8,128)(2,1)}, u32[]{:S(2)}) copy-start(bf16[512,128]{1,0:T(8,128)(2,1)} %param.27) | copy-start | bytes 393220
  9.2 14.1 %copy-start.22 = (bf16[512,128]{1,0:T(8,128)(2,1)S(1)}, bf16[512,128]{1,0:T(8,128)(2,1)}, u32[]{:S(2)}) copy-start(bf16[512,128]{1,0:T(8,128)(2,1)} %param.28) | copy-start | bytes 393220
  9.6 13.5 %copy-start.7 = (f32[512,128]{0,1:T(8,128)}, f32[512,128]{0,1:T(8,128)S(1)}, u32[]{:S(2)}) copy-start(f32[512,128]{0,1:T(8,128)S(1)} %get-tuple-element.357) | copy-start | bytes 786436
  9.6 60.2 %copy-start.9 = (f32[512,128]{0,1:T(8,128)}, f32[512,128]{0,1:T(8,128)S(1)}, u32[]{:S(2)}) copy-start(f32[512,128]{0,1:T(8,128)S(1)} %get-tuple-element.416) | copy-start | bytes 786436
  23.9 5.2 copy-start.15
  23.9 5.2 copy-start.16
  23.9 0.7 copy-start.14
  23.9 2.9 copy-start.13
  74.9 4.5 copy-start.12
  82.4 25.3 %copy-start.18 = (bf16[8,64,2,128]{3,2,1,0:T(2,128)(2,1)S(1)}, bf16[8,64,2,128]{3,2,1,0:T(2,128)(2,1)}, u32[]{:S(2)}) copy-start(bf16[8,64,2,128]{3,2,1,0:T(2,128)(2,1)} %reshape_reshape.8) | copy-start | bytes 786436
  83.2 26.9 %copy-start.26 = (s32[128,2]{0,1:T(2,128)S(1)}, s32[128,2]{0,1:T(2,128)}, u32[]{:S(2)}) copy-start(s32[128,2]{0,1:T(2,128)} %param.38) | copy-start | bytes 3076
  151.2 0.7 copy-start.17
  153.6 1.9 copy-start.10
  155.3 4.0 copy-start.11
  158.3 5.0 copy-start.8
  168.1 1.6 slice-start.1
  168.1 12.2 %copy-start.27 = (f32[256]{0:T(256)S(1)}, f32[256]{0:T(256)}, u32[]{:S(2)}) copy-start(f32[256]{0:T(256)} %param.33) | copy-start | bytes 3076
  178.5 2.1 copy-start.20
  181.5 9.8 %all-to-all-start = ((bf16[4,128,256]{2,1,0:T(8,128)(2,1)}), bf16[4,128,256]{2,1,0:T(8,128)(2,1)S(1)}, u32[]{:S(2)}, u32[]{:S(2)}) async-start(bf16[4,128,256]{2,1,0:T(8,128)(2,1)} %bitcast.62), calls=%async_computation | async-start | bytes 524288 | tf_op jit(solution)/shard_map/all_to_all | solution.py:233
  185.8 117.4 %all-gather.14.cloned.1.call-start = ((), (), s32[]{:S(2)}) async-start(), calls=%async_computation.5 | async-start | bytes 2621440 | tf_op jit(solution)/shard_map/all_gather | solution.py:246
  191.5 3.1 copy-start.19
  191.5 3.1 copy-start.23
  194.6 1.2 copy-start.24
  195.0 0.8 copy-start.5
  196.8 1.0 copy-start.1
  196.8 170.2 %all-gather.12.cloned.1.call-start = ((), (), s32[]{:S(2)}) async-start(), calls=%async_computation.4 | async-start | bytes 7864320 | tf_op jit(solution)/shard_map/all_gather | solution.py:245
  303.1 167.3 %reduce-scatter.2.cloned.1.call-start = ((), (), s32[]{:S(2)}) async-start(), calls=%async_computation.6 | async-start | bytes 10485760 | tf_op jit(solution)/shard_map/reduce_scatter | solution.py:260
  303.2 2.5 copy-start.2
  310.6 61.5 %copy-start.30 = (bf16[1,2048,256]{2,1,0:T(8,128)(2,1)S(1)}, bf16[1,2048,256]{2,1,0:T(8,128)(2,1)}, u32[]{:S(2)}) copy-start(bf16[1,2048,256]{2,1,0:T(8,128)(2,1)} %param.41) | copy-start | bytes 3145732
  367.0 5.1 copy-start.29
  374.2 4.5 copy-start.3
  470.4 1.4 slice-start
  473.4 11.1 %copy-start.28 = (f32[128,2]{0,1:T(2,128)S(1)}, f32[128,2]{0,1:T(2,128)}, u32[]{:S(2)}) copy-start(f32[128,2]{0,1:T(2,128)} %param.39) | copy-start | bytes 3076
  473.4 60.7 %all-to-all-start.2 = ((bf16[64,6,2048]{2,1,0:T(8,128)(2,1)}), bf16[64,6,2048]{2,1,0:T(8,128)(2,1)}, u32[]{:S(2)}, u32[]{:S(2)}) async-start(bf16[64,6,2048]{2,1,0:T(8,128)(2,1)} %reshape.770), calls=%async_computation.3 | async-start | bytes 4194304 | tf_op jit(solution)/shard_map/all_to_all | solution.py:271
  541.4 3.2 copy-start.4
  541.4 3.5 copy-start.6
  541.4 3.5 copy-start.25
Sparse Core Ops, SparseCore 0:
  62.0 81.6 all-gather.15
  196.9 39.1 all-gather.13
  303.2 63.7 all-gather.11
  386.5 83.8 reduce-scatter.1
where the time goes:
time: 557 us; the launch traced here: 552 us
  waiting for transfers between devices  196 us (35%)
  local copies, waits for them, and re-layouts  119 us (21%)
  blocking collectives  103 us (18%)
  matrix products  56.2 us (10%)
  other arithmetic  46.9 us (8%)
  starting transfers between devices  15.4 us (3%)
  between operations  14 us (3%)
    reduce_scatter x1, waiting for transfers between devices, body(): lax.psum_scatter(jnp.concatenate([routed_out, shared_out], axis=1).reshap...  84 us
    all_to_all x1, blocking collectives, body(): lax.all_to_all(fill_slots(normed, routes, experts, capacity), SP, split_a...  66.7 us
    all_gather x1, waiting for transfers between devices, body(): lax.all_gather(arrived.reshape(experts * capacity, model_width), 'tp', ax...  56.5 us
    all_to_all x1, waiting for transfers between devices, body(): lax.all_to_all(routed_done, SP, split_axis=0, concat_axis=0, tiled=True)  49.5 us
    all_gather x3, blocking collectives, gathered_once(): both, at, found = (lax.all_gather(jnp.concatenate(lines), axis), 0, {})  35.8 us
    scatter x2, local copies, waits for them, and re-layouts, fill_slots(): return buffer.at[flat_ids, slot_ids].set(row_data[token_ids])  34.5 us
    dynamic_slice x32, local copies, waits for them, and re-layouts, blockwise(): lax.scan(advance, start_state, (query_in, key_out, value_blocks, block_de...  20.9 us
    dot_general x16, matrix products, advance(): jnp.einsum('jco,jcm->com', key_segment, value_segment)  15.2 us
  transfers between devices with their start and end apart: 6, of which 4 were waited for; matrix products, arithmetic and copies ran while one was open for 21% of the time, Pallas kernels for 0%

commit v1 on v0

v1 whole, which is shorter than its diff:
```python
import functools

import jax
import jax.numpy as jnp
import numpy as np
from jax import lax
from jax.experimental import pallas as pl
from jax.experimental.pallas import tpu as pltpu
from jax.sharding import PartitionSpec as P

KEY_CHANNELS = 64
DV = 128
TOPK = 2
CAP = 6
CHUNK = 128
LANES = 128
EPS = 1e-06
GATE_NORM = 16.0
ROPE_BASE = 10000.0
MESH = pl.DeviceIdType.MESH
NT = (((1,), (1,)), ((), ()))
TN = (((0,), (0,)), ((), ()))
F32 = jnp.float32
BF16 = jnp.bfloat16


def rope_tables(span, devices):
    half = KEY_CHANNELS // 2
    freq = ROPE_BASE ** (-np.arange(half, dtype=np.float64) / half)
    freq = np.tile(freq, LANES // half)
    inner = np.arange(span)[:, None] * freq[None, :]
    outer = (np.arange(devices) * span)[:, None] * freq[None, :]
    inner = np.stack([np.cos(inner), np.sin(inner)]).astype(np.float32)
    outer = np.stack([np.cos(outer), np.sin(outer)], axis=1).astype(np.float32)
    return inner, outer


def attention_kernel(
    groups,
    members,
    q_ref,
    k_ref,
    v_ref,
    g_ref,
    fd_ref,
    bd_ref,
    gain_ref,
    inner_ref,
    outer_ref,
    mixed_ref,
    qs_ref,
    ks_ref,
    out_ref,
    upd_ref,
    half_ref,
    send_ref,
    got_ref,
    back_ref,
    carry_ref,
    mine_ref,
    send_sem,
    recv_sem,
    back_send_sem,
    back_recv_sem,
    mix_send_sem,
    mix_recv_sem,
):
    me = lax.axis_index("sp")
    row = lax.axis_index("tp")
    span = q_ref.shape[0]
    chunks = span // CHUNK
    share = DV // groups
    message = 4 * share

    barrier = pltpu.get_barrier_semaphore()

    def greet(i, c):
        pl.semaphore_signal(
            barrier, inc=1, device_id={"sp": lax.rem(me + i, groups)}, device_id_type=MESH
        )
        return c

    lax.fori_loop(1, groups, greet, 0)
    for i in range(1, members):
        pl.semaphore_signal(
            barrier, inc=1, device_id={"tp": lax.rem(row + i, members)}, device_id_type=MESH
        )

    lane = lax.broadcasted_iota(jnp.int32, (CHUNK, LANES), 1)
    r_id = lax.broadcasted_iota(jnp.int32, (CHUNK, CHUNK), 0)
    c_id = lax.broadcasted_iota(jnp.int32, (CHUNK, CHUNK), 1)
    lower = r_id >= c_id
    upper = r_id <= c_id
    lower_one = jnp.where(lower, 1.0, 0.0).astype(BF16)
    upper_one = jnp.where(upper, 1.0, 0.0).astype(BF16)
    front = (lane % KEY_CHANNELS) < (KEY_CHANNELS // 2)
    first_head = lane < KEY_CHANNELS
    cos_0 = outer_ref[0:1, :]
    sin_0 = outer_ref[1:2, :]

    def log_decay(x):
        return (jnp.minimum(x, 0.0) - jnp.log1p(jnp.exp(-jnp.abs(x)))) * (1.0 / GATE_NORM)

    def cumulate(tri, x):
        high = x.astype(BF16)
        low = (x - high.astype(F32)).astype(BF16)
        return jnp.dot(tri, high, preferred_element_type=F32) + jnp.dot(
            tri, low, preferred_element_type=F32
        )

    for b in range(chunks):
        rows = slice(b * CHUNK, (b + 1) * CHUNK)
        cos_i = inner_ref[0, rows, :]
        sin_i = inner_ref[1, rows, :]
        cosine = cos_0 * cos_i - sin_0 * sin_i
        sine = sin_0 * cos_i + cos_0 * sin_i
        sine = jnp.where(front, -sine, sine)

        def rotated(u):
            swapped = jnp.where(
                front,
                pltpu.roll(u, LANES - KEY_CHANNELS // 2, 1),
                pltpu.roll(u, KEY_CHANNELS // 2, 1),
            )
            return u * cosine + swapped * sine

        q = rotated(q_ref[rows, :].astype(F32) * KEY_CHANNELS ** (-0.5))
        k = rotated(k_ref[rows, :].astype(F32))
        cf = cumulate(lower_one, log_decay(fd_ref[rows, :]))
        cb = cumulate(upper_one, log_decay(bd_ref[rows, :]))
        hf = cf[CHUNK - 1 : CHUNK, :] * 0.5
        hb = cb[0:1, :] * 0.5
        half_ref[2 * b : 2 * b + 1, :] = hf
        half_ref[2 * b + 1 : 2 * b + 2, :] = hb
        qf = q * jnp.exp(cf - hf)
        qb = q * jnp.exp(cb - hb)
        kf = (k * jnp.exp(hf - cf)).astype(BF16)
        kb = (k * jnp.exp(hb - cb)).astype(BF16)
        ks_ref[b, :, 0:LANES] = kf
        ks_ref[b, :, LANES : 2 * LANES] = kb
        qs_ref[b, 0:CHUNK, 0:LANES] = jnp.where(first_head, qf, 0.0).astype(BF16)
        qs_ref[b, 0:CHUNK, LANES : 2 * LANES] = jnp.where(first_head, qb, 0.0).astype(BF16)
        qs_ref[b, CHUNK : 2 * CHUNK, 0:LANES] = jnp.where(first_head, 0.0, qf).astype(BF16)
        qs_ref[b, CHUNK : 2 * CHUNK, LANES : 2 * LANES] = jnp.where(first_head, 0.0, qb).astype(
            BF16
        )
        both = lax.dot_general(
            v_ref[rows, :], ks_ref[b], TN, preferred_element_type=F32
        )
        upd_ref[2 * b] = jnp.where(
            first_head, both[0:DV, 0:LANES], both[DV : 2 * DV, 0:LANES]
        ) * jnp.exp(hf)
        upd_ref[2 * b + 1] = jnp.where(
            first_head, both[0:DV, LANES : 2 * LANES], both[DV : 2 * DV, LANES : 2 * LANES]
        ) * jnp.exp(hb)

    def decay_of(b, d):
        return jnp.exp(half_ref[2 * b + d : 2 * b + d + 1, :] * 2.0)

    total_f = upd_ref[0]
    decay_f = decay_of(0, 0)
    for b in range(1, chunks):
        total_f = total_f * decay_of(b, 0) + upd_ref[2 * b]
        decay_f = decay_f * decay_of(b, 0)
    total_b = upd_ref[2 * (chunks - 1) + 1]
    decay_b = decay_of(chunks - 1, 1)
    for b in reversed(range(chunks - 1)):
        total_b = total_b * decay_of(b, 1) + upd_ref[2 * b + 1]
        decay_b = decay_b * decay_of(b, 1)
    for r in range(share):
        part = slice(r * groups, (r + 1) * groups)
        send_ref[pl.ds(r, groups, stride=message), :] = total_f[part, :]
        send_ref[pl.ds(share + r, groups, stride=message), :] = total_b[part, :]
        send_ref[pl.ds(2 * share + r, groups, stride=message), :] = jnp.broadcast_to(
            decay_f, (groups, LANES)
        )
        send_ref[pl.ds(3 * share + r, groups, stride=message), :] = jnp.broadcast_to(
            decay_b, (groups, LANES)
        )

    pl.semaphore_wait(barrier, groups - 1 + members - 1)

    def block(ref, i):
        return ref.at[pl.ds(pl.multiple_of(i * message, message), message)]

    def half_block(ref, i):
        return ref.at[i]

    def out_copy(peer, i):
        return pltpu.make_async_remote_copy(
            src_ref=block(send_ref, peer),
            dst_ref=block(got_ref, me),
            send_sem=send_sem.at[i],
            recv_sem=recv_sem.at[i],
            device_id={"sp": peer},
            device_id_type=MESH,
        )

    def back_copy(peer, i):
        return pltpu.make_async_remote_copy(
            src_ref=half_block(back_ref, peer),
            dst_ref=half_block(carry_ref, me),
            send_sem=back_send_sem.at[i],
            recv_sem=back_recv_sem.at[i],
            device_id={"sp": peer},
            device_id_type=MESH,
        )

    def offset(i):
        half = lax.div(i + 1, 2)
        return jnp.where(lax.rem(i, 2) == 1, half, groups - half)

    def peer_of(i):
        return lax.rem(me + offset(i), groups)

    def each(action):
        def step(i, c):
            action(i)
            return c

        lax.fori_loop(1, groups, step, 0)

    each(lambda i: out_copy(peer_of(i), offset(i)).start())
    mine = pl.ds(pl.multiple_of(me * message, message), message)
    got_ref[mine, :] = send_ref[mine, :]

    for b in range(chunks):
        rows = slice(b * CHUNK, (b + 1) * CHUNK)
        s_f = lax.dot_general(
            qs_ref[b, :, 0:LANES], ks_ref[b, :, 0:LANES], NT, preferred_element_type=F32
        )
        s_b = lax.dot_general(
            qs_ref[b, :, LANES : 2 * LANES],
            ks_ref[b, :, LANES : 2 * LANES],
            NT,
            preferred_element_type=F32,
        )
        for h in range(2):
            part = slice(h * CHUNK, (h + 1) * CHUNK)
            s = jnp.where(lower, s_f[part], 0.0) + jnp.where(upper, s_b[part], 0.0)
            out_ref[h, rows, :] = jnp.dot(
                s.astype(BF16), v_ref[rows, h * DV : (h + 1) * DV], preferred_element_type=F32
            )

    each(lambda i: out_copy(peer_of(i), offset(i)).wait())

    zero = jnp.zeros((share, LANES), F32)

    def scan(s, carried):
        c_f, c_b = carried
        t = groups - 1 - s
        at_s = pl.multiple_of(s * message, message)
        at_t = pl.multiple_of(t * message, message)
        m_s = got_ref[pl.ds(at_s, message), :]
        m_t = got_ref[pl.ds(at_t, message), :]
        back_ref[s, 0:share, :] = c_f
        back_ref[t, share : 2 * share, :] = c_b
        c_f = c_f * m_s[2 * share : 3 * share] + m_s[0:share]
        c_b = c_b * m_t[3 * share : 4 * share] + m_t[share : 2 * share]
        return c_f, c_b

    lax.fori_loop(0, groups, scan, (zero, zero))
    each(lambda i: back_copy(peer_of(i), offset(i)).start())
    carry_ref[me] = back_ref[me]
    each(lambda i: back_copy(peer_of(i), offset(i)).wait())

    state_f = jnp.concatenate([carry_ref[:, r, :] for r in range(share)], axis=0)
    state_b = jnp.concatenate([carry_ref[:, share + r, :] for r in range(share)], axis=0)
    for b in range(chunks):
        before = state_f
        mine_ref[b, :, 0:LANES] = (
            before * jnp.exp(half_ref[2 * b : 2 * b + 1, :])
        ).astype(BF16)
        state_f = state_f * decay_of(b, 0) + upd_ref[2 * b]
    for b in reversed(range(chunks)):
        mine_ref[b, :, LANES : 2 * LANES] = (
            state_b * jnp.exp(half_ref[2 * b + 1 : 2 * b + 2, :])
        ).astype(BF16)
        state_b = state_b * decay_of(b, 1) + upd_ref[2 * b + 1]

    def mix_copy(i):
        peer = lax.rem(row + i, members)
        return pltpu.make_async_remote_copy(
            src_ref=ks_ref.at[peer],
            dst_ref=mixed_ref.at[row],
            send_sem=mix_send_sem.at[i],
            recv_sem=mix_recv_sem.at[i],
            device_id={"tp": peer},
            device_id_type=MESH,
        )

    for b in range(chunks):
        rows = slice(b * CHUNK, (b + 1) * CHUNK)
        across = lax.dot_general(qs_ref[b], mine_ref[b], NT, preferred_element_type=F32)
        for h in range(2):
            o = out_ref[h, rows, :] + across[h * CHUNK : (h + 1) * CHUNK]
            cols = slice(h * DV, (h + 1) * DV)
            o = o * lax.rsqrt(jnp.mean(o * o, axis=-1, keepdims=True) + EPS)
            g = g_ref[rows, cols].astype(F32)
            o = o * gain_ref[0:1, cols] * (g / (1.0 + jnp.exp(-g)))
            ks_ref[b, :, cols] = o.astype(BF16)
    for i in range(1, members):
        mix_copy(i).start()
    mixed_ref[row] = ks_ref[row]
    for i in range(1, members):
        mix_copy(i).wait()


def attention(mesh, queries, key_rows, values, out_gate, fwd_decay, bwd_decay, head_gain):
    groups, members = mesh.shape["sp"], mesh.shape["tp"]
    span = queries.shape[0]
    chunks = span // CHUNK
    share = DV // groups
    inner, outer = rope_tables(span, groups)
    vmem = pl.BlockSpec(memory_space=pltpu.VMEM)
    outer_row = lax.dynamic_index_in_dim(
        jnp.asarray(outer), lax.axis_index("sp"), 0, keepdims=False
    )
    return pl.pallas_call(
        functools.partial(attention_kernel, groups, members),
        out_shape=jax.ShapeDtypeStruct((members, CHUNK, 2 * DV), BF16),
        in_specs=[vmem] * 9,
        out_specs=vmem,
        scratch_shapes=[
            pltpu.VMEM((chunks, 2 * CHUNK, 2 * LANES), BF16),
            pltpu.VMEM((chunks, CHUNK, 2 * LANES), BF16),
            pltpu.VMEM((2, span, DV), F32),
            pltpu.VMEM((2 * chunks, DV, LANES), F32),
            pltpu.VMEM((2 * chunks, LANES), F32),
            pltpu.VMEM((groups * 4 * share, LANES), F32),
            pltpu.VMEM((groups * 4 * share, LANES), F32),
            pltpu.VMEM((groups, 2 * share, LANES), F32),
            pltpu.VMEM((groups, 2 * share, LANES), F32),
            pltpu.VMEM((chunks, DV, 2 * LANES), BF16),
            pltpu.SemaphoreType.DMA((groups,)),
            pltpu.SemaphoreType.DMA((groups,)),
            pltpu.SemaphoreType.DMA((groups,)),
            pltpu.SemaphoreType.DMA((groups,)),
            pltpu.SemaphoreType.DMA((members,)),
            pltpu.SemaphoreType.DMA((members,)),
        ],
        compiler_params=pltpu.CompilerParams(collective_id=0, has_side_effects=True),
        cost_estimate=pl.CostEstimate(flops=10**10, bytes_accessed=10**8, transcendentals=0),
        name="attention",
    )(
        queries,
        key_rows,
        values,
        out_gate,
        fwd_decay,
        bwd_decay,
        head_gain.reshape(1, -1),
        jnp.asarray(inner),
        outer_row,
    )


def exchange_kernel(groups, src_ref, dst_ref, own_sem, send_sem, recv_sem):
    me = lax.axis_index("sp")
    barrier = pltpu.get_barrier_semaphore()

    def greet(i, c):
        pl.semaphore_signal(
            barrier, inc=1, device_id={"sp": lax.rem(me + i, groups)}, device_id_type=MESH
        )
        return c

    lax.fori_loop(1, groups, greet, 0)
    own = pltpu.make_async_copy(src_ref.at[me], dst_ref.at[me], own_sem)
    own.start()
    pl.semaphore_wait(barrier, groups - 1)

    def copy(i):
        half = lax.div(i + 1, 2)
        shift = jnp.where(lax.rem(i, 2) == 1, half, groups - half)
        peer = lax.rem(me + shift, groups)
        return pltpu.make_async_remote_copy(
            src_ref=src_ref.at[peer],
            dst_ref=dst_ref.at[me],
            send_sem=send_sem.at[shift],
            recv_sem=recv_sem.at[shift],
            device_id={"sp": peer},
            device_id_type=MESH,
        )

    def start(i, c):
        copy(i).start()
        return c

    def finish(i, c):
        copy(i).wait()
        return c

    lax.fori_loop(1, groups, start, 0)
    lax.fori_loop(1, groups, finish, 0)
    own.wait()


def exchange(mesh, array, number):
    groups = mesh.shape["sp"]
    anywhere = pl.BlockSpec(memory_space=pl.ANY)
    return pl.pallas_call(
        functools.partial(exchange_kernel, groups),
        out_shape=jax.ShapeDtypeStruct(array.shape, array.dtype),
        in_specs=[anywhere],
        out_specs=anywhere,
        scratch_shapes=[
            pltpu.SemaphoreType.DMA,
            pltpu.SemaphoreType.DMA((groups,)),
            pltpu.SemaphoreType.DMA((groups,)),
        ],
        compiler_params=pltpu.CompilerParams(collective_id=number, has_side_effects=True),
        cost_estimate=pl.CostEstimate(flops=10**10, bytes_accessed=10**8, transcendentals=0),
        name="exchange",
    )(array)


def normalize(tensor):
    return tensor * lax.rsqrt(jnp.mean(tensor * tensor, axis=-1, keepdims=True) + EPS)


def dot(a, b):
    return jnp.dot(a, b, preferred_element_type=F32)


def silu(x):
    return x / (1.0 + jnp.exp(-x))


def body(
    mesh,
    stream,
    queries,
    key_rows,
    values,
    out_gate,
    fwd_decay,
    bwd_decay,
    head_gain,
    out_proj,
    mix_gain,
    ffn_gain,
    moe_gain,
    routes,
    route_weight,
    expert_gate,
    expert_up,
    expert_down,
    shared_gate,
    shared_up,
    shared_down,
):
    tokens, width = stream.shape
    experts, members = mesh.shape["sp"], mesh.shape["tp"]
    slots = experts * CAP
    gate_all = lax.all_gather(expert_gate[0], "tp", axis=0, tiled=False)
    up_all = lax.all_gather(expert_up[0], "tp", axis=0, tiled=False)
    down_all = lax.all_gather(expert_down[0], "tp", axis=0, tiled=True)

    flat = routes.reshape(-1)
    named = (flat[:, None] == jnp.arange(experts, dtype=jnp.int32)[None, :]).astype(BF16)
    count = tokens * TOPK
    earlier = (
        jnp.arange(count, dtype=jnp.int32)[:, None] > jnp.arange(count, dtype=jnp.int32)[None, :]
    ).astype(BF16)
    slot = jnp.sum(dot(earlier, named) * named.astype(F32), axis=1).astype(jnp.int32)
    place = (flat * CAP + slot).reshape(tokens, TOPK)
    where = jnp.arange(slots, dtype=jnp.int32)
    hit = place[:, :, None] == where[None, None, :]
    put = jnp.any(hit, axis=1).astype(BF16)
    weigh = jnp.sum(jnp.where(hit, route_weight[:, :, None], 0.0), axis=1)
    weigh_high = weigh.astype(BF16)
    weigh_low = (weigh - weigh_high.astype(F32)).astype(BF16)

    mixed = attention(
        mesh, queries, key_rows, values, out_gate, fwd_decay, bwd_decay, head_gain
    )
    mixed, shared_gate, shared_up, shared_down = lax.optimization_barrier(
        (mixed, shared_gate, shared_up, shared_down)
    )
    sgate_all = lax.all_gather(shared_gate, "tp", axis=0, tiled=False)
    sup_all = lax.all_gather(shared_up, "tp", axis=0, tiled=False)
    sdown_all = lax.all_gather(shared_down, "tp", axis=0, tiled=True)
    projected = sum(
        dot(mixed[i], out_proj[i * 2 * DV : (i + 1) * 2 * DV]) for i in range(members)
    )
    residual = (stream.astype(F32) + normalize(projected) * mix_gain).astype(BF16)
    normed = (normalize(residual.astype(F32)) * ffn_gain).astype(BF16)
    filled = lax.dot_general(put, normed, TN, preferred_element_type=F32).astype(BF16)
    lines = CAP * width // LANES
    arrived = exchange(mesh, filled.reshape(experts, lines, LANES), 1).reshape(slots, width)
    hidden = jnp.concatenate(
        [
            (silu(dot(arrived, gate_all[i])) * dot(arrived, up_all[i])).astype(BF16)
            for i in range(members)
        ],
        axis=1,
    )
    answer = dot(hidden, down_all).astype(BF16)
    returned = exchange(mesh, answer.reshape(experts, lines, LANES), 2).reshape(slots, width)
    returned, normed = lax.optimization_barrier((returned, normed))
    shared_hidden = jnp.concatenate(
        [
            (silu(dot(normed, sgate_all[i])) * dot(normed, sup_all[i])).astype(BF16)
            for i in range(members)
        ],
        axis=1,
    )
    mixture = (
        dot(shared_hidden, sdown_all) + dot(weigh_high, returned) + dot(weigh_low, returned)
    )
    return (residual.astype(F32) + normalize(mixture) * moe_gain).astype(BF16)


def solution(mesh):
    placed = (
        P(("sp", "tp"), None),
        P("sp", "tp"),
        P("sp", "tp"),
        P("sp", "tp"),
        P("sp", "tp"),
        P("sp", "tp"),
        P("sp", "tp"),
        P("tp"),
        P(),
        P(),
        P(),
        P(),
        P(("sp", "tp"), None),
        P(("sp", "tp"), None),
        P("sp", None, "tp"),
        P("sp", None, "tp"),
        P("sp", "tp", None),
        P(None, "tp"),
        P(None, "tp"),
        P("tp", None),
    )
    return jax.shard_map(
        functools.partial(body, mesh),
        mesh=mesh,
        in_specs=placed,
        out_specs=P(("sp", "tp"), None),
        check_vma=False,
    )
```

time: 557 us -> 289 us (0.52)
  Pallas kernels: 0 us -> 131 us
  local copies, waits for them, and re-layouts: 119 us -> 12.6 us
  blocking collectives: 103 us -> 0 us
  waiting for transfers between devices: 196 us -> 95.5 us
  other arithmetic: 46.9 us -> 1.88 us
  matrix products: 56.2 us -> 33.8 us
  starting transfers between devices: 15.4 us -> 0.38 us
    pallas_call x0 -> x3, Pallas kernels: none -> 131 us  [the longest x2 87.4 us: exchange(): pl.pallas_call(functools.partial(exchange_kernel, groups), out_shape=jax....]
    reduce_scatter x1 -> x0, waiting for transfers between devices: 84 us -> none  [body(): lax.psum_scatter(jnp.concatenate([routed_out, shared_out], axis=1).reshap...]
    all_to_all x1 -> x0, blocking collectives: 66.7 us -> none  [body(): lax.all_to_all(fill_slots(normed, routes, experts, capacity), SP, split_a...]
    all_to_all x2 -> x0, waiting for transfers between devices: 55 us -> none  [the longest x1 49.5 us: body(): lax.all_to_all(routed_done, SP, split_axis=0, concat_axis=0, tiled=True)]
    all_gather x3 -> x6, waiting for transfers between devices: 56.5 us -> 92.5 us  [the longest x1 45.9 us: body(): down_all = lax.all_gather(expert_down[0], 'tp', axis=0, tiled=True)]
    all_gather x3 -> x0, blocking collectives: 35.8 us -> none  [gathered_once(): both, at, found = (lax.all_gather(jnp.concatenate(lines), axis), 0, {})]
    scatter x2 -> x0, local copies, waits for them, and re-layouts: 34.5 us -> none  [fill_slots(): return buffer.at[flat_ids, slot_ids].set(row_data[token_ids])]
    dot_general x42 -> x26, matrix products: 56.2 us -> 33.8 us  [the longest x25 33.2 us: dot(): return jnp.dot(a, b, preferred_element_type=F32)]
  transfers between devices with their start and end apart: 6 -> 6, of which waited for: 4 -> 4; matrix products, arithmetic and copies ran while one was open for 21% -> 15% of each run, Pallas kernels for 0% -> 45%
where the time goes in v1:
time: 289 us
  Pallas kernels  131 us (45%)
  waiting for transfers between devices  95.5 us (33%)
  matrix products  33.8 us (12%)
  between operations  13.8 us (5%)
  local copies, waits for them, and re-layouts  12.6 us (4%)
    pallas_call x2, Pallas kernels, exchange(): pl.pallas_call(functools.partial(exchange_kernel, groups), out_shape=jax....  87.4 us
    all_gather x1, waiting for transfers between devices, body(): down_all = lax.all_gather(expert_down[0], 'tp', axis=0, tiled=True)  45.9 us
    pallas_call x1, Pallas kernels, attention(): pl.pallas_call(functools.partial(attention_kernel, groups, members), out_...  43.5 us
    dot_general x25, matrix products, dot(): return jnp.dot(a, b, preferred_element_type=F32)  33.2 us
    all_gather x1, waiting for transfers between devices, body(): sdown_all = lax.all_gather(shared_down, 'tp', axis=0, tiled=True)  31.4 us
    all_gather x1, waiting for transfers between devices, body(): sup_all = lax.all_gather(shared_up, 'tp', axis=0, tiled=False)  13.7 us
  transfers between devices with their start and end apart: 6, of which 4 were waited for; matrix products, arithmetic and copies ran while one was open for 15% of the time, Pallas kernels for 45%

profile of v1, /device:TPU:1, one launch (start us, length us, event | category | flops | bytes accessed | tf_op | source)
XLA Modules:
  0.0 288.9 jit_solution(11253906325396726970)
XLA Ops:
  6.5 0.7 all-gather.10.cloned.1.call-update
  7.3 0.7 all-gather.12.cloned.1.call-update
  8.1 0.7 all-gather.16.cloned.1.call-update
  8.8 1.2 dynamic-slice_bitcast_fusion.outer_ref
  10.0 43.5 %attention.1 = bf16[4,128,256]{2,1,0:T(8,128)(2,1)} custom-call(bf16[512,128]{1,0:T(8,128)(2,1)} %q_ref.1, bf16[512,128]{1,0:T(8,128)(2,1)} %k_ref.1, bf16[512,256]{1,0:T(8,128)(2,1)} %v_ref.1, bf16[512,256]{1,0:T(8,128)(2,1)} %g_ref.1, f32[512,128]{1,0:T(8,128)} %fd_ref.1, f32[512,128]{1,0:T(8,128)} %bd_ref.1, f32[1,256]{1,0:T(1,128)} %bitcast.67, ...), custom_call_target="tpu_custom_call" | custom-call | flops 10000000000 | bytes 100000000 | tf_op jit(solution)/shard_map/attention/pallas_call | solution.py:319
  53.7 0.5 all-gather.20.cloned.1.call-update
  54.2 0.2 all-gather.14.cloned.1.call-start
  54.4 0.3 all-gather.14.cloned.1.call-update
  54.8 1.7 fusion.25
  56.5 1.5 convolution_add_fusion.4
  58.1 0.3 convolution_add_fusion.3
  58.5 0.4 multiply_reduce_fusion.1
  58.9 0.6 copy-done.2
  59.5 0.4 fusion.14
  60.1 0.2 fusion.13
  60.9 0.6 convolution_convert_fusion
  61.5 2.1 reshape.54.src_ref
  63.6 43.6 %exchange.2 = bf16[64,96,128]{2,1,0:T(8,128)(2,1)} custom-call(bf16[64,96,128]{2,1,0:T(8,128)(2,1)} %reshape.54.src_ref), custom_call_target="tpu_custom_call" | custom-call | flops 10000000000 | bytes 100000000 | tf_op jit(solution)/shard_map/exchange/pallas_call | solution.py:402
  107.2 2.6 reshape.55
  110.0 2.9 %fusion.21 = f32[384,256]{0,1:T(8,128)} fusion(bf16[384,2048]{1,0:T(8,128)(2,1)S(1)} %reshape.55, bf16[4,2048,256]{2,1,0:T(8,128)(2,1)} %all-gather.10.cloned.1.call-done), kind=kOutput, calls=%fused_computation.45 | convolution fusion | flops 402653184 | bytes 3014656 | tf_op jit(solution)/shard_map/dot_general | solution.py:423
  112.9 2.7 fusion.20
  115.6 1.5 fusion.19
  117.1 0.8 fusion.18
  117.9 1.5 all-gather.12.cloned.1.call-done
  119.4 2.2 fusion.5
  121.6 0.4 copy-done.9
  122.0 1.5 fusion.6
  123.5 1.4 fusion.7
  124.9 1.4 fusion.8
  126.4 45.9 %all-gather.16.cloned.1.call-done = bf16[1,1024,2048]{2,1,0:T(8,128)(2,1)} async-done(((bf16[1,256,2048]{2,1,0:T(8,128)(2,1)}), bf16[1,1024,2048]{2,1,0:T(8,128)(2,1)}) %all-gather.16.cloned.1.call-update) | async-done | bytes 4194320 | tf_op jit(solution)/shard_map/all_gather | solution.py:458
  172.3 4.3 %fusion.2 = bf16[384,2048]{1,0:T(8,128)(2,1)S(1)} fusion(bf16[1,1024,2048]{2,1,0:T(8,128)(2,1)} %all-gather.16.cloned.1.call-done, bf16[384,256]{0,1:T(8,128)(2,1)} %fusion.8, bf16[384,256]{0,1:T(8,128)(2,1)} %fusion.7, bf16[384,256]{0,1:T(8,128)(2,1)} %fusion.6, bf16[384,256]{0,1:T(8,128)(2,1)S(1)} %fusion.5), kind=kOutput, calls=%fused_computation.2 | convolution fusion | flops 1614544896 | bytes 6553600 | tf_op jit(solution)/shard_map/dot_general | solution.py:423
  176.6 2.1 reshape.56.src_ref
  178.8 43.9 %exchange.3 = bf16[64,96,128]{2,1,0:T(8,128)(2,1)} custom-call(bf16[64,96,128]{2,1,0:T(8,128)(2,1)} %reshape.56.src_ref), custom_call_target="tpu_custom_call" | custom-call | flops 10000000000 | bytes 100000000 | tf_op jit(solution)/shard_map/exchange/pallas_call | solution.py:402
  222.6 2.8 reshape.57
  225.5 1.5 fusion.44
  227.0 1.4 fusion.41
  228.4 0.3 fusion.38
  228.8 0.3 fusion.35
  229.1 13.7 %all-gather.20.cloned.1.call-done = bf16[8192,128]{1,0:T(8,128)(2,1)} async-done(((bf16[2048,128]{1,0:T(8,128)(2,1)}), bf16[8192,128]{1,0:T(8,128)(2,1)}) %all-gather.20.cloned.1.call-update) | async-done | bytes 2097168 | tf_op jit(solution)/shard_map/all_gather | solution.py:482
  242.8 1.5 fusion.9
  244.3 1.4 fusion.10
  245.7 0.4 fusion.11
  246.1 0.4 fusion.12
  246.4 31.4 %all-gather.14.cloned.1.call-done = bf16[512,2048]{1,0:T(8,128)(2,1)} async-done(((bf16[128,2048]{1,0:T(8,128)(2,1)}), bf16[512,2048]{1,0:T(8,128)(2,1)}) %all-gather.14.cloned.1.call-update) | async-done | bytes 2097168 | tf_op jit(solution)/shard_map/all_gather | solution.py:483
  277.9 2.1 fusion.47
  279.9 0.4 convolution_add_fusion.1
  280.4 0.5 multiply_reduce_fusion
  281.1 1.0 fusion.17
  (46 shorter events, 1.4 us)
Async XLA Ops:
  6.5 103.4 %all-gather.10.cloned.1.call-start = ((), (), s32[]{:S(2)}) async-start(), calls=%async_computation | async-start | bytes 5242880 | tf_op jit(solution)/shard_map/all_gather | solution.py:456
  7.3 112.1 %all-gather.12.cloned.1.call-start = ((), (), s32[]{:S(2)}) async-start(), calls=%async_computation.1 | async-start | bytes 5242880 | tf_op jit(solution)/shard_map/all_gather | solution.py:457
  8.0 164.3 %all-gather.16.cloned.1.call-start = ((), (), s32[]{:S(2)}) async-start(), calls=%async_computation.3 | async-start | bytes 5242880 | tf_op jit(solution)/shard_map/all_gather | solution.py:458
  8.7 216.7 %all-gather.18.cloned.1.call-start = ((), (), s32[]{:S(2)}) async-start(), calls=%async_computation.4 | async-start | bytes 2621440 | tf_op jit(solution)/shard_map/all_gather | solution.py:481
  53.6 2.9 %copy-start.3 = (bf16[4,128,256]{2,1,0:T(8,128)(2,1)S(1)}, bf16[4,128,256]{2,1,0:T(8,128)(2,1)}, u32[]{:S(2)}) copy-start(bf16[4,128,256]{2,1,0:T(8,128)(2,1)} %attention.1) | copy-start | bytes 786436
  53.6 189.2 %all-gather.20.cloned.1.call-start = ((), (), s32[]{:S(2)}) async-start(), calls=%async_computation.5 | async-start | bytes 2621440 | tf_op jit(solution)/shard_map/all_gather | solution.py:482
  54.2 223.6 %all-gather.14.cloned.1.call-start = ((), (), s32[]{:S(2)}) async-start(), calls=%async_computation.2 | async-start | bytes 2621440 | tf_op jit(solution)/shard_map/all_gather | solution.py:483
  54.8 3.3 %copy-start = (bf16[1024,2048]{1,0:T(8,128)(2,1)S(1)}, bf16[1024,2048]{1,0:T(8,128)(2,1)}, u32[]{:S(2)}) copy-start(bf16[1024,2048]{1,0:T(8,128)(2,1)} %param.30) | copy-start | bytes 12582916
  58.4 1.0 copy-start.2
  58.4 1.0 copy-start.4
  58.4 1.4 copy-start.7
  58.5 2.2 copy-start.5
  107.2 2.6 copy-start.8
  110.0 5.6 %copy-start.10 = (bf16[4,2048,256]{2,1,0:T(8,128)(2,1)S(1)}, bf16[4,2048,256]{2,1,0:T(8,128)(2,1)}, u32[]{:S(2)}) copy-start(bf16[4,2048,256]{2,1,0:T(8,128)(2,1)} %all-gather.10.cloned.1.call-done) | copy-start | bytes 12582916
  119.4 2.6 copy-start.9
  119.4 2.7 copy-start.13
  122.0 1.5 copy-start.12
  225.5 2.9 %copy-start.1 = (bf16[8192,128]{1,0:T(8,128)(2,1)S(1)}, bf16[8192,128]{1,0:T(8,128)(2,1)}, u32[]{:S(2)}) copy-start(bf16[8192,128]{1,0:T(8,128)(2,1)} %all-gather.18.cloned.1.call-done) | copy-start | bytes 6291460
  242.8 2.9 %copy-start.11 = (bf16[8192,128]{1,0:T(8,128)(2,1)S(1)}, bf16[8192,128]{1,0:T(8,128)(2,1)}, u32[]{:S(2)}) copy-start(bf16[8192,128]{1,0:T(8,128)(2,1)} %all-gather.20.cloned.1.call-done) | copy-start | bytes 6291460
  280.4 0.7 copy-start.6
Sparse Core Ops, SparseCore 0:
  9.1 57.2 all-gather.9
  68.2 51.1 all-gather.11
  121.2 51.1 all-gather.15
  174.0 33.6 all-gather.17
  209.4 33.3 all-gather.19
  244.4 33.3 all-gather.13

commit v2 on v1

--- a/solution.py
+++ b/solution.py
@@ -47,7 +47,28 @@
     gain_ref,
     inner_ref,
     outer_ref,
+    stream_ref,
+    proj_hbm,
+    mix_gain_ref,
+    ffn_gain_ref,
+    routes_ref,
+    spread_ref,
+    target_ref,
+    gate_hbm,
+    up_hbm,
+    down_hbm,
+    arrived_ref,
+    residual_ref,
+    normed_ref,
+    put_ref,
+    gate_all,
+    up_all,
+    down_all,
     mixed_ref,
+    proj_ref,
+    projected_ref,
+    stage_ref,
+    filled_ref,
     qs_ref,
     ks_ref,
     out_ref,
@@ -64,9 +85,58 @@
     back_recv_sem,
     mix_send_sem,
     mix_recv_sem,
+    row_send_sem,
+    row_recv_sem,
+    near_send_sem,
+    near_recv_sem,
+    far_send_sem,
+    far_recv_sem,
+    local_sem,
 ):
     me = lax.axis_index("sp")
     row = lax.axis_index("tp")
+    shards = (gate_hbm, up_hbm, down_hbm)
+    wholes = (gate_all, up_all, down_all)
+    sides = (lax.rem(row + 1, members), lax.rem(row + members - 1, members))
+    proj_copy = pltpu.make_async_copy(proj_hbm, proj_ref, local_sem.at[0])
+    proj_copy.start()
+    own_copies = [
+        pltpu.make_async_copy(shards[t], wholes[t].at[3], local_sem.at[1 + t]) for t in range(3)
+    ]
+    for copy in own_copies:
+        copy.start()
+
+    def near_copy(t, side):
+        return pltpu.make_async_remote_copy(
+            src_ref=shards[t],
+            dst_ref=wholes[t].at[side],
+            send_sem=near_send_sem.at[2 * t + side],
+            recv_sem=near_recv_sem.at[2 * t + side],
+            device_id={"tp": sides[side]},
+            device_id_type=MESH,
+        )
+
+    def far_copy(t, side):
+        half = shards[t].shape[0] // 2
+        part = pl.ds(side * half, half)
+        return pltpu.make_async_remote_copy(
+            src_ref=wholes[t].at[side, part],
+            dst_ref=wholes[t].at[2, part],
+            send_sem=far_send_sem.at[2 * t + side],
+            recv_sem=far_recv_sem.at[2 * t + side],
+            device_id={"tp": sides[side]},
+            device_id_type=MESH,
+        )
+
+    def send_near(t):
+        for side in range(2):
+            near_copy(t, side).start()
+
+    def send_far(t):
+        for side in range(2):
+            near_copy(t, side).wait_recv()
+            far_copy(t, side).start()
+
     span = q_ref.shape[0]
     chunks = span // CHUNK
     share = DV // groups
@@ -153,6 +223,9 @@
         upd_ref[2 * b + 1] = jnp.where(
             first_head, both[0:DV, LANES : 2 * LANES], both[DV : 2 * DV, LANES : 2 * LANES]
         ) * jnp.exp(hb)
+        if b == 0:
+            pl.semaphore_wait(barrier, groups - 1 + members - 1)
+            send_near(0)
 
     def decay_of(b, d):
         return jnp.exp(half_ref[2 * b + d : 2 * b + d + 1, :] * 2.0)
@@ -178,8 +251,6 @@
             decay_b, (groups, LANES)
         )
 
-    pl.semaphore_wait(barrier, groups - 1 + members - 1)
-
     def block(ref, i):
         return ref.at[pl.ds(pl.multiple_of(i * message, message), message)]
 
@@ -262,6 +333,7 @@
     lax.fori_loop(0, groups, scan, (zero, zero))
     each(lambda i: back_copy(peer_of(i), offset(i)).start())
     carry_ref[me] = back_ref[me]
+    send_far(0)
     each(lambda i: back_copy(peer_of(i), offset(i)).wait())
 
     state_f = jnp.concatenate([carry_ref[:, r, :] for r in range(share)], axis=0)
@@ -301,27 +373,139 @@
             ks_ref[b, :, cols] = o.astype(BF16)
     for i in range(1, members):
         mix_copy(i).start()
+    send_near(1)
+    send_near(2)
     mixed_ref[row] = ks_ref[row]
+
+    count = normed_ref.shape[0]
+    width = normed_ref.shape[1]
+    lines = width // LANES
+    expert_id = lax.broadcasted_iota(jnp.int32, (count, LANES), 1)
+    token_id = lax.broadcasted_iota(jnp.int32, (count, count), 0)
+    other_id = lax.broadcasted_iota(jnp.int32, (count, count), 1)
+    named = jnp.where(routes_ref[:, 0:1] == expert_id, 1.0, 0.0) + jnp.where(
+        routes_ref[:, 1:2] == expert_id, 1.0, 0.0
+    )
+    earlier = jnp.where(token_id > other_id, 1.0, 0.0).astype(BF16)
+    rank = jnp.dot(earlier, named.astype(BF16), preferred_element_type=F32)
+    ranked = (named * (rank + 1.0)).astype(BF16)
+    spread = jnp.dot(ranked, spread_ref[...], preferred_element_type=F32)
+    put_ref[...] = jnp.where(spread == target_ref[...], 1.0, 0.0).astype(BF16)
+
+    proj_copy.wait()
     for i in range(1, members):
         mix_copy(i).wait()
-
-
-def attention(mesh, queries, key_rows, values, out_gate, fwd_decay, bwd_decay, head_gain):
+    mixed = jnp.concatenate([mixed_ref[i] for i in range(members)], axis=1)
+    step = min(512, width)
+    for n in range(width // step):
+        cols = slice(n * step, (n + 1) * step)
+        projected_ref[:, cols] = jnp.dot(mixed, proj_ref[:, cols], preferred_element_type=F32)
+    for i in range(count // 16):
+        rows = slice(i * 16, (i + 1) * 16)
+        p = projected_ref[rows, :]
+        p = p * lax.rsqrt(jnp.mean(p * p, axis=-1, keepdims=True) + EPS) * mix_gain_ref[...]
+        r = (stream_ref[rows, :].astype(F32) + p).astype(BF16)
+        residual_ref[rows, :] = r
+        r = r.astype(F32)
+        r = r * lax.rsqrt(jnp.mean(r * r, axis=-1, keepdims=True) + EPS) * ffn_gain_ref[...]
+        normed_ref[rows, :] = r.astype(BF16)
+    slots = put_ref.shape[1]
+    for n in range(width // (2 * LANES)):
+        f = lax.dot_general(
+            put_ref[...],
+            normed_ref[:, n * 2 * LANES : (n + 1) * 2 * LANES],
+            TN,
+            preferred_element_type=F32,
+        )
+        stage_ref[pl.ds(2 * n, slots, stride=lines), :] = f[:, 0:LANES]
+        stage_ref[pl.ds(2 * n + 1, slots, stride=lines), :] = f[:, LANES : 2 * LANES]
+    piece = slots * lines // groups
+
+    def narrow(i, c):
+        rows = pl.ds(pl.multiple_of(i * piece, 16), piece)
+        filled_ref[rows, :] = stage_ref[rows, :].astype(BF16)
+        return c
+
+    lax.fori_loop(0, groups, narrow, 0)
+
+    def row_copy(peer, i):
+        return pltpu.make_async_remote_copy(
+            src_ref=filled_ref.at[pl.ds(pl.multiple_of(peer * piece, 16), piece)],
+            dst_ref=arrived_ref.at[pl.ds(pl.multiple_of(me * piece, 16), piece)],
+            send_sem=row_send_sem.at[i],
+            recv_sem=row_recv_sem.at[i],
+            device_id={"sp": peer},
+            device_id_type=MESH,
+        )
+
+    each(lambda i: row_copy(peer_of(i), offset(i)).start())
+    own = pl.ds(pl.multiple_of(me * piece, 16), piece)
+    own_rows = pltpu.make_async_copy(filled_ref.at[own], arrived_ref.at[own], local_sem.at[4])
+    own_rows.start()
+    send_far(1)
+    send_far(2)
+    each(lambda i: row_copy(peer_of(i), offset(i)).wait())
+    for t in range(3):
+        for side in range(2):
+            near_copy(t, side).wait_send()
+            far_copy(t, side).wait()
+    for copy in own_copies:
+        copy.wait()
+    own_rows.wait()
+
+
+def attention(
+    mesh,
+    stream,
+    queries,
+    key_rows,
+    values,
+    out_gate,
+    fwd_decay,
+    bwd_decay,
+    head_gain,
+    out_proj,
+    mix_gain,
+    ffn_gain,
+    routes,
+    gate,
+    up,
+    down,
+):
     groups, members = mesh.shape["sp"], mesh.shape["tp"]
     span = queries.shape[0]
     chunks = span // CHUNK
     share = DV // groups
+    tokens, width = stream.shape
+    slots = groups * CAP
+    lines = width // LANES
     inner, outer = rope_tables(span, groups)
     vmem = pl.BlockSpec(memory_space=pltpu.VMEM)
+    anywhere = pl.BlockSpec(memory_space=pl.ANY)
     outer_row = lax.dynamic_index_in_dim(
         jnp.asarray(outer), lax.axis_index("sp"), 0, keepdims=False
     )
+    spread, target = slot_tables(groups)
+    dma = pltpu.SemaphoreType.DMA
     return pl.pallas_call(
         functools.partial(attention_kernel, groups, members),
-        out_shape=jax.ShapeDtypeStruct((members, CHUNK, 2 * DV), BF16),
-        in_specs=[vmem] * 9,
-        out_specs=vmem,
+        out_shape=(
+            jax.ShapeDtypeStruct((slots * lines, LANES), BF16),
+            jax.ShapeDtypeStruct((tokens, width), BF16),
+            jax.ShapeDtypeStruct((tokens, width), BF16),
+            jax.ShapeDtypeStruct((tokens, slots), BF16),
+            jax.ShapeDtypeStruct((4, *gate.shape), BF16),
+            jax.ShapeDtypeStruct((4, *up.shape), BF16),
+            jax.ShapeDtypeStruct((4, *down.shape), BF16),
+        ),
+        in_specs=[vmem] * 10 + [anywhere] + [vmem] * 5 + [anywhere] * 3,
+        out_specs=(anywhere, vmem, vmem, vmem, anywhere, anywhere, anywhere),
         scratch_shapes=[
+            pltpu.VMEM((members, CHUNK, 2 * DV), BF16),
+            pltpu.VMEM(out_proj.shape, BF16),
+            pltpu.VMEM((tokens, width), F32),
+            pltpu.VMEM((slots * lines, LANES), F32),
+            pltpu.VMEM((slots * lines, LANES), BF16),
             pltpu.VMEM((chunks, 2 * CHUNK, 2 * LANES), BF16),
             pltpu.VMEM((chunks, CHUNK, 2 * LANES), BF16),
             pltpu.VMEM((2, span, DV), F32),
@@ -332,12 +516,19 @@
             pltpu.VMEM((groups, 2 * share, LANES), F32),
             pltpu.VMEM((groups, 2 * share, LANES), F32),
             pltpu.VMEM((chunks, DV, 2 * LANES), BF16),
-            pltpu.SemaphoreType.DMA((groups,)),
-            pltpu.SemaphoreType.DMA((groups,)),
-            pltpu.SemaphoreType.DMA((groups,)),
-            pltpu.SemaphoreType.DMA((groups,)),
-            pltpu.SemaphoreType.DMA((members,)),
-            pltpu.SemaphoreType.DMA((members,)),
+            dma((groups,)),
+            dma((groups,)),
+            dma((groups,)),
+            dma((groups,)),
+            dma((members,)),
+            dma((members,)),
+            dma((groups,)),
+            dma((groups,)),
+            dma((6,)),
+            dma((6,)),
+            dma((6,)),
+            dma((6,)),
+            dma((5,)),
         ],
         compiler_params=pltpu.CompilerParams(collective_id=0, has_side_effects=True),
         cost_estimate=pl.CostEstimate(flops=10**10, bytes_accessed=10**8, transcendentals=0),
@@ -352,11 +543,109 @@
         head_gain.reshape(1, -1),
         jnp.asarray(inner),
         outer_row,
+        stream,
+        out_proj,
+        mix_gain.reshape(1, -1),
+        ffn_gain.reshape(1, -1),
+        routes,
+        jnp.asarray(spread).astype(BF16),
+        jnp.asarray(target),
+        gate,
+        up,
+        down,
     )
 
 
-def exchange_kernel(groups, src_ref, dst_ref, own_sem, send_sem, recv_sem):
+def slot_tables(experts):
+    slot = np.arange(experts * CAP)
+    spread = (np.arange(LANES)[:, None] == slot[None, :] // CAP).astype(np.float32)
+    target = (slot % CAP + 1).astype(np.float32).reshape(1, -1)
+    return spread, target
+
+
+def experts_kernel(x_ref, gate_ref, up_ref, down_ref, out_ref, acc_ref):
+    q = pl.program_id(0)
+    x = x_ref[...]
+    g = jnp.dot(x, gate_ref[0], preferred_element_type=F32)
+    u = jnp.dot(x, up_ref[0], preferred_element_type=F32)
+    h = (g / (1.0 + jnp.exp(-g)) * u).astype(BF16)
+    width = out_ref.shape[1]
+    step = min(512, width)
+    for n in range(width // step):
+        cols = slice(n * step, (n + 1) * step)
+        part = jnp.dot(h, down_ref[0, :, cols], preferred_element_type=F32)
+
+        @pl.when(q == 0)
+        def _():
+            acc_ref[:, cols] = part
+
+        @pl.when(q > 0)
+        def _():
+            acc_ref[:, cols] += part
+
+    @pl.when(q == pl.num_programs(0) - 1)
+    def _():
+        out_ref[...] = acc_ref[...].astype(BF16)
+
+
+def expert_rows(x, gate, up, down):
+    number = gate.shape[0]
+    whole = pl.BlockSpec(x.shape, lambda q: (0, 0))
+    return pl.pallas_call(
+        experts_kernel,
+        out_shape=jax.ShapeDtypeStruct(x.shape, BF16),
+        grid=(number,),
+        in_specs=[
+            whole,
+            pl.BlockSpec((1, *gate.shape[1:]), lambda q: (q, 0, 0)),
+            pl.BlockSpec((1, *up.shape[1:]), lambda q: (q, 0, 0)),
+            pl.BlockSpec((1, *down.shape[1:]), lambda q: (q, 0, 0)),
+        ],
+        out_specs=whole,
+        scratch_shapes=[pltpu.VMEM(x.shape, F32)],
+        name="experts",
+    )(x, gate, up, down)
+
+
+def return_kernel(
+    groups,
+    members,
+    answer_ref,
+    normed_ref,
+    residual_ref,
+    put_ref,
+    routes_ref,
+    weight_ref,
+    spread_ref,
+    moe_gain_ref,
+    gate_ref,
+    up_ref,
+    down_ref,
+    out_ref,
+    back_ref,
+    stage_ref,
+    rows_ref,
+    total_ref,
+    gate_all,
+    up_all,
+    down_all,
+    row_send_sem,
+    row_recv_sem,
+    near_send_sem,
+    near_recv_sem,
+    far_send_sem,
+    far_recv_sem,
+    twin_send_sem,
+    twin_recv_sem,
+    local_sem,
+):
     me = lax.axis_index("sp")
+    row = lax.axis_index("tp")
+    core = lax.rem(me, 2)
+    twin = me + 1 - 2 * core
+    sides = (lax.rem(row + 1, members), lax.rem(row + members - 1, members))
+    shards = (gate_ref, up_ref, down_ref)
+    wholes = (gate_all, up_all, down_all)
     barrier = pltpu.get_barrier_semaphore()
 
     def greet(i, c):
@@ -366,65 +655,217 @@
         return c
 
     lax.fori_loop(1, groups, greet, 0)
-    own = pltpu.make_async_copy(src_ref.at[me], dst_ref.at[me], own_sem)
-    own.start()
-    pl.semaphore_wait(barrier, groups - 1)
-
-    def copy(i):
+    for side in range(2):
+        pl.semaphore_signal(barrier, inc=1, device_id={"tp": sides[side]}, device_id_type=MESH)
+    slots = put_ref.shape[1]
+    count, width = normed_ref.shape
+    lines = width // LANES
+    piece = slots * lines // groups
+    own = pl.ds(pl.multiple_of(me * piece, 16), piece)
+    own_rows = pltpu.make_async_copy(answer_ref.at[own], back_ref.at[own], local_sem.at[0])
+    own_rows.start()
+    pl.semaphore_wait(barrier, groups - 1 + 2)
+
+    def offset(i):
         half = lax.div(i + 1, 2)
-        shift = jnp.where(lax.rem(i, 2) == 1, half, groups - half)
-        peer = lax.rem(me + shift, groups)
+        return jnp.where(lax.rem(i, 2) == 1, half, groups - half)
+
+    def row_copy(i):
+        peer = lax.rem(me + offset(i), groups)
         return pltpu.make_async_remote_copy(
-            src_ref=src_ref.at[peer],
-            dst_ref=dst_ref.at[me],
-            send_sem=send_sem.at[shift],
-            recv_sem=recv_sem.at[shift],
+            src_ref=answer_ref.at[pl.ds(pl.multiple_of(peer * piece, 16), piece)],
+            dst_ref=back_ref.at[own],
+            send_sem=row_send_sem.at[offset(i)],
+            recv_sem=row_recv_sem.at[offset(i)],
             device_id={"sp": peer},
             device_id_type=MESH,
         )
 
-    def start(i, c):
-        copy(i).start()
+    def each(action):
+        def step(i, c):
+            action(i)
+            return c
+
+        lax.fori_loop(1, groups, step, 0)
+
+    each(lambda i: row_copy(i).start())
+
+    def half_of(t):
+        h = shards[t].shape[0] // 2
+        return pl.ds(pl.multiple_of(core * h, 16), h)
+
+    def quarter_of(t, side):
+        h = shards[t].shape[0] // 2
+        return pl.ds(pl.multiple_of(core * h + side * (h // 2), 16), h // 2)
+
+    def near_copy(t, side):
+        return pltpu.make_async_remote_copy(
+            src_ref=shards[t].at[half_of(t)],
+            dst_ref=wholes[t].at[side, half_of(t)],
+            send_sem=near_send_sem.at[2 * t + side],
+            recv_sem=near_recv_sem.at[2 * t + side],
+            device_id={"tp": sides[side]},
+            device_id_type=MESH,
+        )
+
+    def far_copy(t, side):
+        return pltpu.make_async_remote_copy(
+            src_ref=wholes[t].at[side, quarter_of(t, side)],
+            dst_ref=wholes[t].at[2, quarter_of(t, side)],
+            send_sem=far_send_sem.at[2 * t + side],
+            recv_sem=far_recv_sem.at[2 * t + side],
+            device_id={"tp": sides[side]},
+            device_id_type=MESH,
+        )
+
+    def twin_half(t):
+        h = shards[t].shape[0] // 2
+        return pl.ds(pl.multiple_of((1 - core) * h, 16), h)
+
+    def twin_copy(t, k, part):
+        return pltpu.make_async_remote_copy(
+            src_ref=wholes[t].at[k, part],
+            dst_ref=wholes[t].at[k, part],
+            send_sem=twin_send_sem.at[3 * t + k],
+            recv_sem=twin_recv_sem.at[3 * t + k],
+            device_id={"sp": twin},
+            device_id_type=MESH,
+        )
+
+    for t in range(3):
+        for side in range(2):
+            near_copy(t, side).start()
+
+    expert_id = lax.broadcasted_iota(jnp.int32, (count, LANES), 1)
+    weigh = jnp.where(routes_ref[:, 0:1] == expert_id, weight_ref[:, 0:1], 0.0) + jnp.where(
+        routes_ref[:, 1:2] == expert_id, weight_ref[:, 1:2], 0.0
+    )
+    high = weigh.astype(BF16)
+    low = (weigh - high.astype(F32)).astype(BF16)
+    put = put_ref[...].astype(F32)
+    high = (jnp.dot(high, spread_ref[...], preferred_element_type=F32) * put).astype(BF16)
+    low = (jnp.dot(low, spread_ref[...], preferred_element_type=F32) * put).astype(BF16)
+
+    step = min(512, width)
+
+    def shared(gate, up, down, first):
+        x = normed_ref[...]
+        g = jnp.dot(x, gate[...], preferred_element_type=F32)
+        u = jnp.dot(x, up[...], preferred_element_type=F32)
+        h = (g / (1.0 + jnp.exp(-g)) * u).astype(BF16)
+        for n in range(width // step):
+            cols = slice(n * step, (n + 1) * step)
+            part = jnp.dot(h, down[:, cols], preferred_element_type=F32)
+            if first:
+                total_ref[:, cols] = part
+            else:
+                total_ref[:, cols] += part
+
+    shared(gate_ref, up_ref, down_ref, True)
+    for t in range(3):
+        for side in range(2):
+            near_copy(t, side).wait_recv()
+            far_copy(t, side).start()
+            twin_copy(t, side, half_of(t)).start()
+    for t in range(3):
+        for side in range(2):
+            far_copy(t, side).wait_recv()
+        twin_copy(t, 2, half_of(t)).start()
+    for k in range(3):
+        for t in range(3):
+            twin_copy(t, k, twin_half(t)).wait_recv()
+        shared(gate_all.at[k], up_all.at[k], down_all.at[k], False)
+    for t in range(3):
+        for side in range(2):
+            near_copy(t, side).wait_send()
+            far_copy(t, side).wait_send()
+        for k in range(3):
+            twin_copy(t, k, half_of(t)).wait_send()
+
+    own_rows.wait()
+    each(lambda i: row_copy(i).wait())
+
+    def widen(i, c):
+        rows = pl.ds(pl.multiple_of(i * piece, 16), piece)
+        stage_ref[rows, :] = back_ref[rows, :].astype(F32)
         return c
 
-    def finish(i, c):
-        copy(i).wait()
-        return c
-
-    lax.fori_loop(1, groups, start, 0)
-    lax.fori_loop(1, groups, finish, 0)
-    own.wait()
-
-
-def exchange(mesh, array, number):
-    groups = mesh.shape["sp"]
+    lax.fori_loop(0, groups, widen, 0)
+    for n in range(lines):
+        rows_ref[:, n * LANES : (n + 1) * LANES] = stage_ref[
+            pl.ds(n, slots, stride=lines), :
+        ].astype(BF16)
+    for n in range(width // step):
+        cols = slice(n * step, (n + 1) * step)
+        total_ref[:, cols] += jnp.dot(
+            high, rows_ref[:, cols], preferred_element_type=F32
+        ) + jnp.dot(low, rows_ref[:, cols], preferred_element_type=F32)
+    for i in range(count // 16):
+        rows = slice(i * 16, (i + 1) * 16)
+        m = total_ref[rows, :]
+        m = m * lax.rsqrt(jnp.mean(m * m, axis=-1, keepdims=True) + EPS) * moe_gain_ref[...]
+        out_ref[rows, :] = (residual_ref[rows, :].astype(F32) + m).astype(BF16)
+
+
+def returned(
+    mesh,
+    answer,
+    normed,
+    residual,
+    put,
+    routes,
+    route_weight,
+    moe_gain,
+    shared_gate,
+    shared_up,
+    shared_down,
+):
+    groups, members = mesh.shape["sp"], mesh.shape["tp"]
+    tokens, width = normed.shape
+    slots = groups * CAP
+    spread, _ = slot_tables(groups)
+    vmem = pl.BlockSpec(memory_space=pltpu.VMEM)
     anywhere = pl.BlockSpec(memory_space=pl.ANY)
+    dma = pltpu.SemaphoreType.DMA
     return pl.pallas_call(
-        functools.partial(exchange_kernel, groups),
-        out_shape=jax.ShapeDtypeStruct(array.shape, array.dtype),
-        in_specs=[anywhere],
-        out_specs=anywhere,
+        functools.partial(return_kernel, groups, members),
+        out_shape=jax.ShapeDtypeStruct((tokens, width), BF16),
+        in_specs=[anywhere] + [vmem] * 10,
+        out_specs=vmem,
         scratch_shapes=[
-            pltpu.SemaphoreType.DMA,
-            pltpu.SemaphoreType.DMA((groups,)),
-            pltpu.SemaphoreType.DMA((groups,)),
+            pltpu.VMEM(answer.shape, BF16),
+            pltpu.VMEM(answer.shape, F32),
+            pltpu.VMEM((slots, width), BF16),
+            pltpu.VMEM((tokens, width), F32),
+            pltpu.VMEM((3, *shared_gate.shape), BF16),
+            pltpu.VMEM((3, *shared_up.shape), BF16),
+            pltpu.VMEM((3, *shared_down.shape), BF16),
+            dma((groups,)),
+            dma((groups,)),
+            dma((6,)),
+            dma((6,)),
+            dma((6,)),
+            dma((6,)),
+            dma((9,)),
+            dma((9,)),
+            dma((1,)),
         ],
-        compiler_params=pltpu.CompilerParams(collective_id=number, has_side_effects=True),
+        compiler_params=pltpu.CompilerParams(collective_id=1, has_side_effects=True),
         cost_estimate=pl.CostEstimate(flops=10**10, bytes_accessed=10**8, transcendentals=0),
-        name="exchange",
-    )(array)
-
-
-def normalize(tensor):
-    return tensor * lax.rsqrt(jnp.mean(tensor * tensor, axis=-1, keepdims=True) + EPS)
-
-
-def dot(a, b):
-    return jnp.dot(a, b, preferred_element_type=F32)
-
-
-def silu(x):
-    return x / (1.0 + jnp.exp(-x))
+        name="returned",
+    )(
+        answer,
+        normed,
+        residual,
+        put,
+        routes,
+        route_weight,
+        jnp.asarray(spread).astype(BF16),
+        moe_gain.reshape(1, -1),
+        shared_gate,
+        shared_up,
+        shared_down,
+    )
 
 
 def body(
@@ -450,66 +891,40 @@
     shared_up,
     shared_down,
 ):
-    tokens, width = stream.shape
-    experts, members = mesh.shape["sp"], mesh.shape["tp"]
-    slots = experts * CAP
-    gate_all = lax.all_gather(expert_gate[0], "tp", axis=0, tiled=False)
-    up_all = lax.all_gather(expert_up[0], "tp", axis=0, tiled=False)
-    down_all = lax.all_gather(expert_down[0], "tp", axis=0, tiled=True)
-
-    flat = routes.reshape(-1)
-    named = (flat[:, None] == jnp.arange(experts, dtype=jnp.int32)[None, :]).astype(BF16)
-    count = tokens * TOPK
-    earlier = (
-        jnp.arange(count, dtype=jnp.int32)[:, None] > jnp.arange(count, dtype=jnp.int32)[None, :]
-    ).astype(BF16)
-    slot = jnp.sum(dot(earlier, named) * named.astype(F32), axis=1).astype(jnp.int32)
-    place = (flat * CAP + slot).reshape(tokens, TOPK)
-    where = jnp.arange(slots, dtype=jnp.int32)
-    hit = place[:, :, None] == where[None, None, :]
-    put = jnp.any(hit, axis=1).astype(BF16)
-    weigh = jnp.sum(jnp.where(hit, route_weight[:, :, None], 0.0), axis=1)
-    weigh_high = weigh.astype(BF16)
-    weigh_low = (weigh - weigh_high.astype(F32)).astype(BF16)
-
-    mixed = attention(
-        mesh, queries, key_rows, values, out_gate, fwd_decay, bwd_decay, head_gain
+    width = stream.shape[1]
+    slots = mesh.shape["sp"] * CAP
+    arrived, residual, normed, put, gate, up, down = attention(
+        mesh,
+        stream,
+        queries,
+        key_rows,
+        values,
+        out_gate,
+        fwd_decay,
+        bwd_decay,
+        head_gain,
+        out_proj,
+        mix_gain,
+        ffn_gain,
+        routes,
+        expert_gate[0],
+        expert_up[0],
+        expert_down[0],
     )
-    mixed, shared_gate, shared_up, shared_down = lax.optimization_barrier(
-        (mixed, shared_gate, shared_up, shared_down)
+    answer = expert_rows(arrived.reshape(slots, width), gate, up, down)
+    return returned(
+        mesh,
+        answer.reshape(slots * width // LANES, LANES),
+        normed,
+        residual,
+        put,
+        routes,
+        route_weight,
+        moe_gain,
+        shared_gate,
+        shared_up,
+        shared_down,
     )
-    sgate_all = lax.all_gather(shared_gate, "tp", axis=0, tiled=False)
-    sup_all = lax.all_gather(shared_up, "tp", axis=0, tiled=False)
-    sdown_all = lax.all_gather(shared_down, "tp", axis=0, tiled=True)
-    projected = sum(
-        dot(mixed[i], out_proj[i * 2 * DV : (i + 1) * 2 * DV]) for i in range(members)
-    )
-    residual = (stream.astype(F32) + normalize(projected) * mix_gain).astype(BF16)
-    normed = (normalize(residual.astype(F32)) * ffn_gain).astype(BF16)
-    filled = lax.dot_general(put, normed, TN, preferred_element_type=F32).astype(BF16)
-    lines = CAP * width // LANES
-    arrived = exchange(mesh, filled.reshape(experts, lines, LANES), 1).reshape(slots, width)
-    hidden = jnp.concatenate(
-        [
-            (silu(dot(arrived, gate_all[i])) * dot(arrived, up_all[i])).astype(BF16)
-            for i in range(members)
-        ],
-        axis=1,
-    )
-    answer = dot(hidden, down_all).astype(BF16)
-    returned = exchange(mesh, answer.reshape(experts, lines, LANES), 2).reshape(slots, width)
-    returned, normed = lax.optimization_barrier((returned, normed))
-    shared_hidden = jnp.concatenate(
-        [
-            (silu(dot(normed, sgate_all[i])) * dot(normed, sup_all[i])).astype(BF16)
-            for i in range(members)
-        ],
-        axis=1,
-    )
-    mixture = (
-        dot(shared_hidden, sdown_all) + dot(weigh_high, returned) + dot(weigh_low, returned)
-    )
-    return (residual.astype(F32) + normalize(mixture) * moe_gain).astype(BF16)
 
 
 def solution(mesh):

time: 289 us -> 200 us (0.69)
  waiting for transfers between devices: 95.5 us -> 0 us
  Pallas kernels: 131 us -> 187 us
  matrix products: 33.8 us -> 0 us
  between operations: 13.8 us -> 0.02 us
    all_gather x6 -> x0, waiting for transfers between devices: 92.5 us -> none  [the longest x1 45.9 us: body(): down_all = lax.all_gather(expert_down[0], 'tp', axis=0, tiled=True)]
    pallas_call x1, Pallas kernels: 43.5 us -> 126 us  [attention(): pl.pallas_call(functools.partial(attention_kernel, groups, members), out_...]
    dot_general x26 -> x0, matrix products: 33.8 us -> none  [the longest x25 33.2 us: dot(): return jnp.dot(a, b, preferred_element_type=F32)]
    pallas_call x2, Pallas kernels: 87.4 us -> 61.2 us  [the longest x1 48.4 us: returned(): pl.pallas_call(functools.partial(return_kernel, groups, members), out_sha...]
    unnamed x6 -> x0, waiting for transfers between devices: 2.98 us -> none
    reshape x4 -> x2, local copies, waits for them, and re-layouts: 9.61 us -> 7.47 us  [the longest x1 3.76 us: body(): answer.reshape(slots * width // LANES, LANES)]
  transfers between devices with their start and end apart: 6 -> 0, of which waited for: 4 -> 0; matrix products, arithmetic and copies ran while one was open for 15% -> 0% of each run, Pallas kernels for 45% -> 0%
where the time goes in v2:
time: 200 us
  Pallas kernels  187 us (94%)
  local copies, waits for them, and re-layouts  12.8 us (6%)
    pallas_call x1, Pallas kernels, attention(): pl.pallas_call(functools.partial(attention_kernel, groups, members), out_...  126 us
    pallas_call x1, Pallas kernels, returned(): pl.pallas_call(functools.partial(return_kernel, groups, members), out_sha...  48.4 us
    pallas_call x1, Pallas kernels, expert_rows(): pl.pallas_call(experts_kernel, out_shape=jax.ShapeDtypeStruct(x.shape, BF...  12.8 us
    unnamed x5, local copies, waits for them, and re-layouts  4.03 us

profile of v2, /device:TPU:1, one launch (start us, length us, event | category | flops | bytes accessed | tf_op | source)
XLA Modules:
  0.0 200.2 jit_solution(11234227460403230204)
XLA Ops:
  0.0 1.3 dynamic-slice_bitcast_fusion.outer_ref
  1.3 1.4 copy.26.routes_ref
  2.7 126.1 %attention.1 = (bf16[6144,128]{1,0:T(8,128)(2,1)}, bf16[128,2048]{1,0:T(8,128)(2,1)}, bf16[128,2048]{1,0:T(8,128)(2,1)}, bf16[128,384]{1,0:T(8,128)(2,1)}, bf16[...) custom-call(bf16[512,128]{1,0:T(8,128)(2,1)} %q_ref.1, ...), custom_call_target="tpu_custom_call" | custom-call | flops 10000000000 | bytes 100000000 | tf_op jit(solution)/shard_map/attention/pallas_call | solution.py:490
  128.8 3.7 %reshape.21.x_ref = bf16[384,2048]{1,0:T(8,128)(2,1)} reshape(bf16[6144,128]{1,0:T(8,128)(2,1)} %get-tuple-element.12) | data formatting | bytes 3145728 | tf_op jit(solution)/shard_map/reshape | solution.py:914
  132.5 0.0 copy-start
  132.5 12.8 %experts.1 = bf16[384,2048]{1,0:T(8,128)(2,1)} custom-call(bf16[384,2048]{1,0:T(8,128)(2,1)} %reshape.21.x_ref, bf16[4,2048,256]{2,1,0:T(8,128)(2,1)} %get-tuple-element.13.gate_ref, bf16[4,2048,256]{2,1,0:T(8,128)(2,1)} %get-tuple-element.14.up_ref, bf16[4,256,2048]{2,1,0:T(8,128)(2,1)} %get-tuple-element.15.down_ref), custom_call_target="tpu_custom_call" | custom-call | tf_op jit(solution)/shard_map/experts/pallas_call | solution.py:594
  145.4 3.8 %reshape.22.answer_ref = bf16[6144,128]{1,0:T(8,128)(2,1)} reshape(bf16[384,2048]{1,0:T(8,128)(2,1)} %experts.1) | data formatting | bytes 3145728 | tf_op jit(solution)/shard_map/reshape | solution.py:917
  149.1 0.0 copy-done
  149.1 0.7 copy.28.weight_ref
  149.9 48.4 %returned.1 = bf16[128,2048]{1,0:T(8,128)(2,1)} custom-call(bf16[6144,128]{1,0:T(8,128)(2,1)} %reshape.22.answer_ref, bf16[128,2048]{1,0:T(8,128)(2,1)} %get-tuple-element.16.normed_ref, bf16[128,2048]{1,0:T(8,128)(2,1)} %get-tuple-element.17.residual_ref, bf16[128,384]{1,0:T(8,128)(2,1)} %get-tuple-element.18.put_ref, s32[128,2]{1,0:T(8,128)} %copy.26.routes_ref, ...), custom_call_target="tpu_custom_call" | custom-call | flops 10000000000 | bytes 100000000 | tf_op jit(solution)/shard_map/returned/pallas_call | solution.py:830
  198.3 1.9 copy.30
Async XLA Ops:
  132.5 16.6 %copy-start = (f32[128,2]{0,1:T(2,128)S(1)}, f32[128,2]{0,1:T(2,128)}, u32[]{:S(2)}) copy-start(f32[128,2]{0,1:T(2,128)} %param.38) | copy-start | bytes 3076

commit v3 on v1

--- a/solution.py
+++ b/solution.py
@@ -35,7 +35,7 @@
     return inner, outer
 
 
-def attention_kernel(
+def layer_kernel(
     groups,
     members,
     q_ref,
@@ -47,7 +47,40 @@
     gain_ref,
     inner_ref,
     outer_ref,
+    stream_ref,
+    mix_gain_ref,
+    ffn_gain_ref,
+    moe_gain_ref,
+    routes_ref,
+    weight_ref,
+    spread_ref,
+    target_ref,
+    sgate_ref,
+    sup_ref,
+    sdown_ref,
+    proj_hbm,
+    gate_hbm,
+    up_hbm,
+    down_hbm,
+    updated_ref,
+    proj_ref,
+    gate_all,
+    up_all,
+    down_all,
+    sgate_all,
+    sup_all,
+    sdown_all,
     mixed_ref,
+    total_ref,
+    residual_ref,
+    normed_ref,
+    put_ref,
+    stage_ref,
+    filled_ref,
+    arrived_ref,
+    back_ref,
+    x_ref,
+    hidden_ref,
     qs_ref,
     ks_ref,
     out_ref,
@@ -55,7 +88,7 @@
     half_ref,
     send_ref,
     got_ref,
-    back_ref,
+    back_state_ref,
     carry_ref,
     mine_ref,
     send_sem,
@@ -64,13 +97,32 @@
     back_recv_sem,
     mix_send_sem,
     mix_recv_sem,
+    row_send_sem,
+    row_recv_sem,
+    near_send_sem,
+    near_recv_sem,
+    far_send_sem,
+    far_recv_sem,
+    twin_send_sem,
+    twin_recv_sem,
+    local_sem,
 ):
     me = lax.axis_index("sp")
     row = lax.axis_index("tp")
+    core = lax.rem(me, 2)
+    twin = me + 1 - 2 * core
     span = q_ref.shape[0]
     chunks = span // CHUNK
     share = DV // groups
     message = 4 * share
+    count, width = stream_ref.shape
+    lines = width // LANES
+    slots = put_ref.shape[0]
+    half_lines = lines // 2
+    half_rows = slots * half_lines
+    piece = half_rows // groups
+    inner_width = gate_hbm.shape[1]
+    sides = (lax.rem(row + 1, members), lax.rem(row + members - 1, members))
 
     barrier = pltpu.get_barrier_semaphore()
 
@@ -84,6 +136,104 @@
     for i in range(1, members):
         pl.semaphore_signal(
             barrier, inc=1, device_id={"tp": lax.rem(row + i, members)}, device_id_type=MESH
+        )
+
+    own_down = pl.ds(0, inner_width)
+    local_copies = [
+        pltpu.make_async_copy(proj_hbm, proj_ref, local_sem.at[0]),
+        pltpu.make_async_copy(gate_hbm, gate_all.at[0], local_sem.at[1]),
+        pltpu.make_async_copy(up_hbm, up_all.at[0], local_sem.at[2]),
+        pltpu.make_async_copy(down_hbm, down_all.at[own_down], local_sem.at[3]),
+    ]
+    for copy in local_copies:
+        copy.start()
+
+    half_width = width // 2
+
+    def place(t, slot, start, size):
+        if t < 2:
+            whole = (gate_all, up_all)[t]
+            return whole.at[slot, pl.ds(start, size)]
+        cols = pl.ds((t - 2) * half_width, half_width)
+        return down_all.at[pl.ds(slot * inner_width + start, size), cols]
+
+    def shard(t):
+        if t < 2:
+            return (gate_hbm, up_hbm)[t]
+        return down_hbm.at[:, pl.ds((t - 2) * half_width, half_width)]
+
+    def depth(t):
+        return width if t < 2 else inner_width
+
+    def near_copy(t, side):
+        return pltpu.make_async_remote_copy(
+            src_ref=shard(t),
+            dst_ref=place(t, 1 + side, 0, depth(t)),
+            send_sem=near_send_sem.at[2 * t + side],
+            recv_sem=near_recv_sem.at[2 * t + side],
+            device_id={"tp": sides[side]},
+            device_id_type=MESH,
+        )
+
+    def far_copy(t, side):
+        h = depth(t) // 2
+        return pltpu.make_async_remote_copy(
+            src_ref=place(t, 1 + side, side * h, h),
+            dst_ref=place(t, 3, side * h, h),
+            send_sem=far_send_sem.at[2 * t + side],
+            recv_sem=far_recv_sem.at[2 * t + side],
+            device_id={"tp": sides[side]},
+            device_id_type=MESH,
+        )
+
+    def send_near(t):
+        for side in range(2):
+            near_copy(t, side).start()
+
+    def send_far(t):
+        for side in range(2):
+            near_copy(t, side).wait_recv()
+            far_copy(t, side).start()
+
+    shared_own = (sgate_ref, sup_ref, sdown_ref)
+    shared_all = (sgate_all, sup_all, sdown_all)
+
+    def half_of(t, who):
+        h = shared_own[t].shape[0] // 2
+        return pl.ds(pl.multiple_of(who * h, 16), h)
+
+    def quarter_of(t, side):
+        h = shared_own[t].shape[0] // 2
+        return pl.ds(pl.multiple_of(core * h + side * (h // 2), 16), h // 2)
+
+    def shared_near(t, side):
+        return pltpu.make_async_remote_copy(
+            src_ref=shared_own[t].at[half_of(t, core)],
+            dst_ref=shared_all[t].at[side, half_of(t, core)],
+            send_sem=near_send_sem.at[8 + 2 * t + side],
+            recv_sem=near_recv_sem.at[8 + 2 * t + side],
+            device_id={"tp": sides[side]},
+            device_id_type=MESH,
+        )
+
+    def shared_far(t, side):
+        return pltpu.make_async_remote_copy(
+            src_ref=shared_all[t].at[side, quarter_of(t, side)],
+            dst_ref=shared_all[t].at[2, quarter_of(t, side)],
+            send_sem=far_send_sem.at[8 + 2 * t + side],
+            recv_sem=far_recv_sem.at[8 + 2 * t + side],
+            device_id={"tp": sides[side]},
+            device_id_type=MESH,
+        )
+
+    def twin_copy(t, k, part):
+        return pltpu.make_async_remote_copy(
+            src_ref=shared_all[t].at[k, part],
+            dst_ref=shared_all[t].at[k, part],
+            send_sem=twin_send_sem.at[3 * t + k],
+            recv_sem=twin_recv_sem.at[3 * t + k],
+            device_id={"sp": twin},
+            device_id_type=MESH,
         )
 
     lane = lax.broadcasted_iota(jnp.int32, (CHUNK, LANES), 1)
@@ -95,8 +245,8 @@
     upper_one = jnp.where(upper, 1.0, 0.0).astype(BF16)
     front = (lane % KEY_CHANNELS) < (KEY_CHANNELS // 2)
     first_head = lane < KEY_CHANNELS
-    cos_0 = outer_ref[0:1, :]
-    sin_0 = outer_ref[1:2, :]
+    cos_0 = outer_ref[me, 0:1, :]
+    sin_0 = outer_ref[me, 1:2, :]
 
     def log_decay(x):
         return (jnp.minimum(x, 0.0) - jnp.log1p(jnp.exp(-jnp.abs(x)))) * (1.0 / GATE_NORM)
@@ -153,6 +303,9 @@
         upd_ref[2 * b + 1] = jnp.where(
             first_head, both[0:DV, LANES : 2 * LANES], both[DV : 2 * DV, LANES : 2 * LANES]
         ) * jnp.exp(hb)
+        if b == 0:
+            pl.semaphore_wait(barrier, groups - 1 + members - 1)
+            send_near(0)
 
     def decay_of(b, d):
         return jnp.exp(half_ref[2 * b + d : 2 * b + d + 1, :] * 2.0)
@@ -178,8 +331,6 @@
             decay_b, (groups, LANES)
         )
 
-    pl.semaphore_wait(barrier, groups - 1 + members - 1)
-
     def block(ref, i):
         return ref.at[pl.ds(pl.multiple_of(i * message, message), message)]
 
@@ -198,7 +349,7 @@
 
     def back_copy(peer, i):
         return pltpu.make_async_remote_copy(
-            src_ref=half_block(back_ref, peer),
+            src_ref=half_block(back_state_ref, peer),
             dst_ref=half_block(carry_ref, me),
             send_sem=back_send_sem.at[i],
             recv_sem=back_recv_sem.at[i],
@@ -253,15 +404,16 @@
         at_t = pl.multiple_of(t * message, message)
         m_s = got_ref[pl.ds(at_s, message), :]
         m_t = got_ref[pl.ds(at_t, message), :]
-        back_ref[s, 0:share, :] = c_f
-        back_ref[t, share : 2 * share, :] = c_b
+        back_state_ref[s, 0:share, :] = c_f
+        back_state_ref[t, share : 2 * share, :] = c_b
         c_f = c_f * m_s[2 * share : 3 * share] + m_s[0:share]
         c_b = c_b * m_t[3 * share : 4 * share] + m_t[share : 2 * share]
         return c_f, c_b
 
     lax.fori_loop(0, groups, scan, (zero, zero))
     each(lambda i: back_copy(peer_of(i), offset(i)).start())
-    carry_ref[me] = back_ref[me]
+    carry_ref[me] = back_state_ref[me]
+    send_far(0)
     each(lambda i: back_copy(peer_of(i), offset(i)).wait())
 
     state_f = jnp.concatenate([carry_ref[:, r, :] for r in range(share)], axis=0)
@@ -301,130 +453,198 @@
             ks_ref[b, :, cols] = o.astype(BF16)
     for i in range(1, members):
         mix_copy(i).start()
+    send_near(1)
+    send_near(2)
     mixed_ref[row] = ks_ref[row]
+
+    expert_id = lax.broadcasted_iota(jnp.int32, (LANES, count), 0)
+    earlier_id = lax.broadcasted_iota(jnp.int32, (count, count), 0)
+    token_id = lax.broadcasted_iota(jnp.int32, (count, count), 1)
+    first_named = routes_ref[0:1, :] == expert_id
+    second_named = routes_ref[1:2, :] == expert_id
+    named = jnp.where(first_named, 1.0, 0.0) + jnp.where(second_named, 1.0, 0.0)
+    earlier = jnp.where(earlier_id < token_id, 1.0, 0.0).astype(BF16)
+    rank = jnp.dot(named.astype(BF16), earlier, preferred_element_type=F32)
+    ranked = (named * (rank + 1.0)).astype(BF16)
+    spread = jnp.dot(spread_ref[...], ranked, preferred_element_type=F32)
+    put_ref[...] = jnp.where(spread == target_ref[...], 1.0, 0.0).astype(BF16)
+
+    local_copies[0].wait()
     for i in range(1, members):
         mix_copy(i).wait()
-
-
-def attention(mesh, queries, key_rows, values, out_gate, fwd_decay, bwd_decay, head_gain):
-    groups, members = mesh.shape["sp"], mesh.shape["tp"]
-    span = queries.shape[0]
-    chunks = span // CHUNK
-    share = DV // groups
-    inner, outer = rope_tables(span, groups)
-    vmem = pl.BlockSpec(memory_space=pltpu.VMEM)
-    outer_row = lax.dynamic_index_in_dim(
-        jnp.asarray(outer), lax.axis_index("sp"), 0, keepdims=False
-    )
-    return pl.pallas_call(
-        functools.partial(attention_kernel, groups, members),
-        out_shape=jax.ShapeDtypeStruct((members, CHUNK, 2 * DV), BF16),
-        in_specs=[vmem] * 9,
-        out_specs=vmem,
-        scratch_shapes=[
-            pltpu.VMEM((chunks, 2 * CHUNK, 2 * LANES), BF16),
-            pltpu.VMEM((chunks, CHUNK, 2 * LANES), BF16),
-            pltpu.VMEM((2, span, DV), F32),
-            pltpu.VMEM((2 * chunks, DV, LANES), F32),
-            pltpu.VMEM((2 * chunks, LANES), F32),
-            pltpu.VMEM((groups * 4 * share, LANES), F32),
-            pltpu.VMEM((groups * 4 * share, LANES), F32),
-            pltpu.VMEM((groups, 2 * share, LANES), F32),
-            pltpu.VMEM((groups, 2 * share, LANES), F32),
-            pltpu.VMEM((chunks, DV, 2 * LANES), BF16),
-            pltpu.SemaphoreType.DMA((groups,)),
-            pltpu.SemaphoreType.DMA((groups,)),
-            pltpu.SemaphoreType.DMA((groups,)),
-            pltpu.SemaphoreType.DMA((groups,)),
-            pltpu.SemaphoreType.DMA((members,)),
-            pltpu.SemaphoreType.DMA((members,)),
-        ],
-        compiler_params=pltpu.CompilerParams(collective_id=0, has_side_effects=True),
-        cost_estimate=pl.CostEstimate(flops=10**10, bytes_accessed=10**8, transcendentals=0),
-        name="attention",
-    )(
-        queries,
-        key_rows,
-        values,
-        out_gate,
-        fwd_decay,
-        bwd_decay,
-        head_gain.reshape(1, -1),
-        jnp.asarray(inner),
-        outer_row,
-    )
-
-
-def exchange_kernel(groups, src_ref, dst_ref, own_sem, send_sem, recv_sem):
-    me = lax.axis_index("sp")
-    barrier = pltpu.get_barrier_semaphore()
-
-    def greet(i, c):
-        pl.semaphore_signal(
-            barrier, inc=1, device_id={"sp": lax.rem(me + i, groups)}, device_id_type=MESH
-        )
-        return c
-
-    lax.fori_loop(1, groups, greet, 0)
-    own = pltpu.make_async_copy(src_ref.at[me], dst_ref.at[me], own_sem)
-    own.start()
-    pl.semaphore_wait(barrier, groups - 1)
-
-    def copy(i):
-        half = lax.div(i + 1, 2)
-        shift = jnp.where(lax.rem(i, 2) == 1, half, groups - half)
-        peer = lax.rem(me + shift, groups)
-        return pltpu.make_async_remote_copy(
-            src_ref=src_ref.at[peer],
-            dst_ref=dst_ref.at[me],
-            send_sem=send_sem.at[shift],
-            recv_sem=recv_sem.at[shift],
+    mixed = jnp.concatenate([mixed_ref[i] for i in range(members)], axis=1)
+    step = min(512, width)
+    for n in range(width // step):
+        cols = slice(n * step, (n + 1) * step)
+        total_ref[:, cols] = jnp.dot(mixed, proj_ref[:, cols], preferred_element_type=F32)
+    for i in range(count // 16):
+        rows = slice(i * 16, (i + 1) * 16)
+        p = total_ref[rows, :]
+        p = p * lax.rsqrt(jnp.mean(p * p, axis=-1, keepdims=True) + EPS) * mix_gain_ref[...]
+        r = (stream_ref[rows, :].astype(F32) + p).astype(BF16)
+        residual_ref[rows, :] = r
+        r = r.astype(F32)
+        r = r * lax.rsqrt(jnp.mean(r * r, axis=-1, keepdims=True) + EPS) * ffn_gain_ref[...]
+        normed_ref[rows, :] = r.astype(BF16)
+
+    def piece_of(part, i):
+        return pl.ds(pl.multiple_of(part * half_rows + i * piece, 16), piece)
+
+    def row_copy(src, dst, base, part, i):
+        peer = peer_of(i)
+        return pltpu.make_async_remote_copy(
+            src_ref=src.at[piece_of(part, peer)],
+            dst_ref=dst.at[piece_of(part, me)],
+            send_sem=row_send_sem.at[base + part, offset(i)],
+            recv_sem=row_recv_sem.at[base + part, offset(i)],
             device_id={"sp": peer},
             device_id_type=MESH,
         )
 
-    def start(i, c):
-        copy(i).start()
-        return c
-
-    def finish(i, c):
-        copy(i).wait()
-        return c
-
-    lax.fori_loop(1, groups, start, 0)
-    lax.fori_loop(1, groups, finish, 0)
-    own.wait()
-
-
-def exchange(mesh, array, number):
-    groups = mesh.shape["sp"]
-    anywhere = pl.BlockSpec(memory_space=pl.ANY)
-    return pl.pallas_call(
-        functools.partial(exchange_kernel, groups),
-        out_shape=jax.ShapeDtypeStruct(array.shape, array.dtype),
-        in_specs=[anywhere],
-        out_specs=anywhere,
-        scratch_shapes=[
-            pltpu.SemaphoreType.DMA,
-            pltpu.SemaphoreType.DMA((groups,)),
-            pltpu.SemaphoreType.DMA((groups,)),
-        ],
-        compiler_params=pltpu.CompilerParams(collective_id=number, has_side_effects=True),
-        cost_estimate=pl.CostEstimate(flops=10**10, bytes_accessed=10**8, transcendentals=0),
-        name="exchange",
-    )(array)
-
-
-def normalize(tensor):
-    return tensor * lax.rsqrt(jnp.mean(tensor * tensor, axis=-1, keepdims=True) + EPS)
-
-
-def dot(a, b):
-    return jnp.dot(a, b, preferred_element_type=F32)
-
-
-def silu(x):
-    return x / (1.0 + jnp.exp(-x))
+    def put_lines(part, line, array):
+        for k in range(array.shape[1] // LANES):
+            at = pl.ds(part * half_rows + line + k, slots, stride=half_lines)
+            stage_ref[at, :] = array[:, k * LANES : (k + 1) * LANES]
+
+    def narrow(part):
+        def one(i, c):
+            filled_ref[piece_of(part, i), :] = stage_ref[piece_of(part, i), :].astype(BF16)
+            return c
+
+        lax.fori_loop(0, groups, one, 0)
+
+    def get_lines(dst, part):
+        for k in range(half_lines):
+            at = pl.ds(part * half_rows + k, slots, stride=half_lines)
+            n = part * half_lines + k
+            dst[:, n * LANES : (n + 1) * LANES] = stage_ref[at, :].astype(BF16)
+
+    def send_rows(dst, base, part):
+        each(lambda i: row_copy(filled_ref, dst, base, part, i).start())
+
+    def take_rows(dst, base, part):
+        own = piece_of(part, me)
+        stage_ref[own, :] = filled_ref[own, :].astype(F32)
+
+        def one(i):
+            row_copy(filled_ref, dst, base, part, i).wait()
+            came = piece_of(part, lax.rem(me + groups - offset(i), groups))
+            stage_ref[came, :] = dst[came, :].astype(F32)
+
+        each(one)
+
+    wide = min(2 * LANES, half_width)
+    for part in range(2):
+        for n in range(half_width // wide):
+            cols = pl.ds(part * half_width + n * wide, wide)
+            f = jnp.dot(put_ref[...], normed_ref[:, cols], preferred_element_type=F32)
+            put_lines(part, n * (wide // LANES), f)
+        narrow(part)
+        send_rows(arrived_ref, 0, part)
+
+    send_far(1)
+    send_near(3)
+    send_far(2)
+    for t in range(3):
+        for side in range(2):
+            shared_near(t, side).start()
+    for part in range(2):
+        take_rows(arrived_ref, 0, part)
+    for part in range(2):
+        get_lines(x_ref, part)
+    for copy in local_copies[1:]:
+        copy.wait()
+
+    def hide(slot):
+        g = jnp.dot(x_ref[...], gate_all[slot], preferred_element_type=F32)
+        u = jnp.dot(x_ref[...], up_all[slot], preferred_element_type=F32)
+        hidden_ref[:, slot * inner_width : (slot + 1) * inner_width] = (
+            g / (1.0 + jnp.exp(-g)) * u
+        ).astype(BF16)
+
+    for slot in range(3):
+        hide(slot)
+    send_far(3)
+    for t in range(2):
+        for side in range(2):
+            far_copy(t, side).wait_recv()
+    hide(3)
+    for part in range(2):
+        for side in range(2):
+            far_copy(2 + part, side).wait_recv()
+        for n in range(half_width // wide):
+            cols = pl.ds(part * half_width + n * wide, wide)
+            f = jnp.dot(hidden_ref[...], down_all[:, cols], preferred_element_type=F32)
+            put_lines(part, n * (wide // LANES), f)
+        narrow(part)
+        send_rows(back_ref, 2, part)
+
+    first_weight = jnp.where(first_named, weight_ref[0:1, :], 0.0)
+    weigh = first_weight + jnp.where(second_named, weight_ref[1:2, :], 0.0)
+    high = weigh.astype(BF16)
+    low = (weigh - high.astype(F32)).astype(BF16)
+    put = put_ref[...].astype(F32)
+    high = (jnp.dot(spread_ref[...], high, preferred_element_type=F32) * put).astype(BF16)
+    low = (jnp.dot(spread_ref[...], low, preferred_element_type=F32) * put).astype(BF16)
+
+    def shared(gate, up, down, first):
+        x = normed_ref[...]
+        g = jnp.dot(x, gate[...], preferred_element_type=F32)
+        u = jnp.dot(x, up[...], preferred_element_type=F32)
+        h = (g / (1.0 + jnp.exp(-g)) * u).astype(BF16)
+        for n in range(width // step):
+            cols = slice(n * step, (n + 1) * step)
+            more = jnp.dot(h, down[:, cols], preferred_element_type=F32)
+            if first:
+                total_ref[:, cols] = more
+            else:
+                total_ref[:, cols] += more
+
+    for t in range(3):
+        for side in range(2):
+            shared_near(t, side).wait_recv()
+            shared_far(t, side).start()
+            twin_copy(t, side, half_of(t, core)).start()
+    shared(sgate_ref, sup_ref, sdown_ref, True)
+    for t in range(3):
+        for side in range(2):
+            shared_far(t, side).wait_recv()
+        twin_copy(t, 2, half_of(t, core)).start()
+    for k in range(3):
+        for t in range(3):
+            twin_copy(t, k, half_of(t, 1 - core)).wait_recv()
+        shared(sgate_all.at[k], sup_all.at[k], sdown_all.at[k], False)
+    for t in range(4):
+        for side in range(2):
+            near_copy(t, side).wait_send()
+            far_copy(t, side).wait_send()
+    for t in range(3):
+        for side in range(2):
+            shared_near(t, side).wait_send()
+            shared_far(t, side).wait_send()
+        for k in range(3):
+            twin_copy(t, k, half_of(t, core)).wait_send()
+
+    for part in range(2):
+        take_rows(back_ref, 2, part)
+        get_lines(x_ref, part)
+        for n in range(half_width // wide):
+            cols = pl.ds(part * half_width + n * wide, wide)
+            total_ref[:, cols] += lax.dot_general(
+                high, x_ref[:, cols], TN, preferred_element_type=F32
+            ) + lax.dot_general(low, x_ref[:, cols], TN, preferred_element_type=F32)
+    for i in range(count // 16):
+        rows = slice(i * 16, (i + 1) * 16)
+        m = total_ref[rows, :]
+        m = m * lax.rsqrt(jnp.mean(m * m, axis=-1, keepdims=True) + EPS) * moe_gain_ref[...]
+        updated_ref[rows, :] = (residual_ref[rows, :].astype(F32) + m).astype(BF16)
+
+
+def slot_tables(experts):
+    slot = np.arange(experts * CAP)
+    spread = (slot[:, None] // CAP == np.arange(LANES)[None, :]).astype(np.float32)
+    target = (slot % CAP + 1).astype(np.float32).reshape(-1, 1)
+    return spread, target
 
 
 def body(
@@ -450,66 +670,101 @@
     shared_up,
     shared_down,
 ):
+    groups, members = mesh.shape["sp"], mesh.shape["tp"]
+    span = queries.shape[0]
+    chunks = span // CHUNK
+    share = DV // groups
     tokens, width = stream.shape
-    experts, members = mesh.shape["sp"], mesh.shape["tp"]
-    slots = experts * CAP
-    gate_all = lax.all_gather(expert_gate[0], "tp", axis=0, tiled=False)
-    up_all = lax.all_gather(expert_up[0], "tp", axis=0, tiled=False)
-    down_all = lax.all_gather(expert_down[0], "tp", axis=0, tiled=True)
-
-    flat = routes.reshape(-1)
-    named = (flat[:, None] == jnp.arange(experts, dtype=jnp.int32)[None, :]).astype(BF16)
-    count = tokens * TOPK
-    earlier = (
-        jnp.arange(count, dtype=jnp.int32)[:, None] > jnp.arange(count, dtype=jnp.int32)[None, :]
-    ).astype(BF16)
-    slot = jnp.sum(dot(earlier, named) * named.astype(F32), axis=1).astype(jnp.int32)
-    place = (flat * CAP + slot).reshape(tokens, TOPK)
-    where = jnp.arange(slots, dtype=jnp.int32)
-    hit = place[:, :, None] == where[None, None, :]
-    put = jnp.any(hit, axis=1).astype(BF16)
-    weigh = jnp.sum(jnp.where(hit, route_weight[:, :, None], 0.0), axis=1)
-    weigh_high = weigh.astype(BF16)
-    weigh_low = (weigh - weigh_high.astype(F32)).astype(BF16)
-
-    mixed = attention(
-        mesh, queries, key_rows, values, out_gate, fwd_decay, bwd_decay, head_gain
+    slots = groups * CAP
+    lines = width // LANES
+    inner_width = expert_gate.shape[2]
+    inner, outer = rope_tables(span, groups)
+    spread, target = slot_tables(groups)
+    vmem = pl.BlockSpec(memory_space=pltpu.VMEM)
+    anywhere = pl.BlockSpec(memory_space=pl.ANY)
+    dma = pltpu.SemaphoreType.DMA
+    mem = pltpu.VMEM
+    return pl.pallas_call(
+        functools.partial(layer_kernel, groups, members),
+        out_shape=jax.ShapeDtypeStruct((tokens, width), BF16),
+        in_specs=[vmem] * 20 + [anywhere] * 4,
+        out_specs=vmem,
+        scratch_shapes=[
+            mem(out_proj.shape, BF16),
+            mem((members, width, inner_width), BF16),
+            mem((members, width, inner_width), BF16),
+            mem((members * inner_width, width), BF16),
+            mem((3, *shared_gate.shape), BF16),
+            mem((3, *shared_up.shape), BF16),
+            mem((3, *shared_down.shape), BF16),
+            mem((members, CHUNK, 2 * DV), BF16),
+            mem((tokens, width), F32),
+            mem((tokens, width), BF16),
+            mem((tokens, width), BF16),
+            mem((slots, tokens), BF16),
+            mem((slots * lines, LANES), F32),
+            mem((slots * lines, LANES), BF16),
+            mem((slots * lines, LANES), BF16),
+            mem((slots * lines, LANES), BF16),
+            mem((slots, width), BF16),
+            mem((slots, members * inner_width), BF16),
+            mem((chunks, 2 * CHUNK, 2 * LANES), BF16),
+            mem((chunks, CHUNK, 2 * LANES), BF16),
+            mem((2, span, DV), F32),
+            mem((2 * chunks, DV, LANES), F32),
+            mem((2 * chunks, LANES), F32),
+            mem((groups * 4 * share, LANES), F32),
+            mem((groups * 4 * share, LANES), F32),
+            mem((groups, 2 * share, LANES), F32),
+            mem((groups, 2 * share, LANES), F32),
+            mem((chunks, DV, 2 * LANES), BF16),
+            dma((groups,)),
+            dma((groups,)),
+            dma((groups,)),
+            dma((groups,)),
+            dma((members,)),
+            dma((members,)),
+            dma((4, groups)),
+            dma((4, groups)),
+            dma((14,)),
+            dma((14,)),
+            dma((14,)),
+            dma((14,)),
+            dma((9,)),
+            dma((9,)),
+            dma((4,)),
+        ],
+        compiler_params=pltpu.CompilerParams(
+            collective_id=0, has_side_effects=True, vmem_limit_bytes=60 * 2**20
+        ),
+        cost_estimate=pl.CostEstimate(flops=10**10, bytes_accessed=10**8, transcendentals=0),
+        name="layer",
+    )(
+        queries,
+        key_rows,
+        values,
+        out_gate,
+        fwd_decay,
+        bwd_decay,
+        head_gain.reshape(1, -1),
+        jnp.asarray(inner),
+        jnp.asarray(outer),
+        stream,
+        mix_gain.reshape(1, -1),
+        ffn_gain.reshape(1, -1),
+        moe_gain.reshape(1, -1),
+        routes.T,
+        route_weight.T,
+        jnp.asarray(spread).astype(BF16),
+        jnp.asarray(target),
+        shared_gate,
+        shared_up,
+        shared_down,
+        out_proj,
+        expert_gate[0],
+        expert_up[0],
+        expert_down[0],
     )
-    mixed, shared_gate, shared_up, shared_down = lax.optimization_barrier(
-        (mixed, shared_gate, shared_up, shared_down)
-    )
-    sgate_all = lax.all_gather(shared_gate, "tp", axis=0, tiled=False)
-    sup_all = lax.all_gather(shared_up, "tp", axis=0, tiled=False)
-    sdown_all = lax.all_gather(shared_down, "tp", axis=0, tiled=True)
-    projected = sum(
-        dot(mixed[i], out_proj[i * 2 * DV : (i + 1) * 2 * DV]) for i in range(members)
-    )
-    residual = (stream.astype(F32) + normalize(projected) * mix_gain).astype(BF16)
-    normed = (normalize(residual.astype(F32)) * ffn_gain).astype(BF16)
-    filled = lax.dot_general(put, normed, TN, preferred_element_type=F32).astype(BF16)
-    lines = CAP * width // LANES
-    arrived = exchange(mesh, filled.reshape(experts, lines, LANES), 1).reshape(slots, width)
-    hidden = jnp.concatenate(
-        [
-            (silu(dot(arrived, gate_all[i])) * dot(arrived, up_all[i])).astype(BF16)
-            for i in range(members)
-        ],
-        axis=1,
-    )
-    answer = dot(hidden, down_all).astype(BF16)
-    returned = exchange(mesh, answer.reshape(experts, lines, LANES), 2).reshape(slots, width)
-    returned, normed = lax.optimization_barrier((returned, normed))
-    shared_hidden = jnp.concatenate(
-        [
-            (silu(dot(normed, sgate_all[i])) * dot(normed, sup_all[i])).astype(BF16)
-            for i in range(members)
-        ],
-        axis=1,
-    )
-    mixture = (
-        dot(shared_hidden, sdown_all) + dot(weigh_high, returned) + dot(weigh_low, returned)
-    )
-    return (residual.astype(F32) + normalize(mixture) * moe_gain).astype(BF16)
 
 
 def solution(mesh):

time: 289 us -> 170 us (0.59)
  waiting for transfers between devices: 95.5 us -> 0 us
  Pallas kernels: 131 us -> 168 us
  matrix products: 33.8 us -> 0 us
  between operations: 13.8 us -> 0.01 us
  local copies, waits for them, and re-layouts: 12.6 us -> 1.88 us
    all_gather x6 -> x0, waiting for transfers between devices: 92.5 us -> none  [the longest x1 45.9 us: body(): down_all = lax.all_gather(expert_down[0], 'tp', axis=0, tiled=True)]
    pallas_call x3 -> x1, Pallas kernels: 131 us -> 168 us  [body(): pl.pallas_call(functools.partial(layer_kernel, groups, members), out_shap...]
    dot_general x26 -> x0, matrix products: 33.8 us -> none  [the longest x25 33.2 us: dot(): return jnp.dot(a, b, preferred_element_type=F32)]
    reshape x4 -> x0, local copies, waits for them, and re-layouts: 9.61 us -> none  [the longest x1 2.82 us: body(): exchange(mesh, answer.reshape(experts, lines, LANES), 2)]
    unnamed x6 -> x0, waiting for transfers between devices: 2.98 us -> none
  transfers between devices with their start and end apart: 6 -> 0, of which waited for: 4 -> 0; matrix products, arithmetic and copies ran while one was open for 15% -> 0% of each run, Pallas kernels for 45% -> 0%
where the time goes in v3:
time: 170 us
  Pallas kernels  168 us (99%)
  local copies, waits for them, and re-layouts  1.88 us (1%)
    pallas_call x1, Pallas kernels, body(): pl.pallas_call(functools.partial(layer_kernel, groups, members), out_shap...  168 us

profile of v3, /device:TPU:1, one launch (start us, length us, event | category | flops | bytes accessed | tf_op | source)
XLA Modules:
  0.0 169.6 jit_solution(12703777105366796366)
XLA Ops:
  0.0 167.8 %layer.1 = bf16[128,2048]{1,0:T(8,128)(2,1)} custom-call(bf16[512,128]{1,0:T(8,128)(2,1)} %q_ref.1, bf16[512,128]{1,0:T(8,128)(2,1)} %k_ref.1, bf16[512,256]{1,0:T(8,128)(2,1)} %v_ref.1, bf16[512,256]{1,0:T(8,128)(2,1)} %g_ref.1, f32[512,128]{1,0:T(8,128)} %fd_ref.1, f32[512,128]{1,0:T(8,128)} %bd_ref.1, f32[1,256]{1,0:T(1,128)} %bitcast.15, ...), custom_call_target="tpu_custom_call" | custom-call | flops 10000000000 | bytes 100000000 | tf_op jit(solution)/shard_map/layer/pallas_call | solution.py:687
  167.8 1.9 %copy.26 = bf16[128,2048]{1,0:T(8,128)(2,1)} copy(bf16[128,2048]{1,0:T(8,128)(2,1)} %layer.1) | data formatting | bytes 1048576

commit v4 on v3

--- a/solution.py
+++ b/solution.py
@@ -103,6 +103,8 @@
     near_recv_sem,
     far_send_sem,
     far_recv_sem,
+    cross_send_sem,
+    cross_recv_sem,
     twin_send_sem,
     twin_recv_sem,
     local_sem,
@@ -175,13 +177,14 @@
             device_id_type=MESH,
         )
 
-    def far_copy(t, side):
-        h = depth(t) // 2
-        return pltpu.make_async_remote_copy(
-            src_ref=place(t, 1 + side, side * h, h),
-            dst_ref=place(t, 3, side * h, h),
-            send_sem=far_send_sem.at[2 * t + side],
-            recv_sem=far_recv_sem.at[2 * t + side],
+    def far_copy(t, side, sub):
+        h = depth(t) // 4
+        start = (2 * side + sub) * h
+        return pltpu.make_async_remote_copy(
+            src_ref=place(t, 1 + side, start, h),
+            dst_ref=place(t, 3, start, h),
+            send_sem=far_send_sem.at[4 * t + 2 * side + sub],
+            recv_sem=far_recv_sem.at[4 * t + 2 * side + sub],
             device_id={"tp": sides[side]},
             device_id_type=MESH,
         )
@@ -190,41 +193,72 @@
         for side in range(2):
             near_copy(t, side).start()
 
-    def send_far(t):
+    def take_near(t):
         for side in range(2):
             near_copy(t, side).wait_recv()
-            far_copy(t, side).start()
+
+    def send_far(t, subs=(0, 1)):
+        for side in range(2):
+            for sub in subs:
+                far_copy(t, side, sub).start()
 
     shared_own = (sgate_ref, sup_ref, sdown_ref)
     shared_all = (sgate_all, sup_all, sdown_all)
+
+    crew = min(8, groups)
+    seat = lax.rem(me, crew)
+    stops = crew // 2
+    turn = core * stops + lax.div(seat, 2)
 
     def half_of(t, who):
         h = shared_own[t].shape[0] // 2
         return pl.ds(pl.multiple_of(who * h, 16), h)
 
-    def quarter_of(t, side):
-        h = shared_own[t].shape[0] // 2
-        return pl.ds(pl.multiple_of(core * h + side * (h // 2), 16), h // 2)
+    def share_of(t):
+        e = shared_own[t].shape[0] // crew
+        return pl.ds(pl.multiple_of(turn * e, 16), e)
 
     def shared_near(t, side):
         return pltpu.make_async_remote_copy(
-            src_ref=shared_own[t].at[half_of(t, core)],
-            dst_ref=shared_all[t].at[side, half_of(t, core)],
+            src_ref=shared_own[t].at[share_of(t)],
+            dst_ref=shared_all[t].at[side, share_of(t)],
             send_sem=near_send_sem.at[8 + 2 * t + side],
             recv_sem=near_recv_sem.at[8 + 2 * t + side],
             device_id={"tp": sides[side]},
             device_id_type=MESH,
         )
 
+    def part_of(t, k, side):
+        if t < 2:
+            e = shared_own[t].shape[0] // crew
+            start = pl.multiple_of(turn * e + side * (e // 2), 16)
+            return shared_all[t].at[k, pl.ds(start, e // 2)]
+        return shared_all[t].at[k, share_of(t), pl.ds(side * half_width, half_width)]
+
     def shared_far(t, side):
         return pltpu.make_async_remote_copy(
-            src_ref=shared_all[t].at[side, quarter_of(t, side)],
-            dst_ref=shared_all[t].at[2, quarter_of(t, side)],
-            send_sem=far_send_sem.at[8 + 2 * t + side],
-            recv_sem=far_recv_sem.at[8 + 2 * t + side],
+            src_ref=part_of(t, side, side),
+            dst_ref=part_of(t, 2, side),
+            send_sem=far_send_sem.at[16 + 2 * t + side],
+            recv_sem=far_recv_sem.at[16 + 2 * t + side],
             device_id={"tp": sides[side]},
             device_id_type=MESH,
         )
+
+    def cross_copy(t, k, n):
+        return pltpu.make_async_remote_copy(
+            src_ref=shared_all[t].at[k, share_of(t)],
+            dst_ref=shared_all[t].at[k, share_of(t)],
+            send_sem=cross_send_sem.at[(3 * t + k) * stops + n],
+            recv_sem=cross_recv_sem.at[(3 * t + k) * stops + n],
+            device_id={"sp": me - seat + lax.rem(seat + 2 * n, crew)},
+            device_id_type=MESH,
+        )
+
+    def send_cross(k):
+        for t in range(3):
+            for n in range(1, stops):
+                cross_copy(t, k, n).start()
 
     def twin_copy(t, k, part):
         return pltpu.make_async_remote_copy(
@@ -305,6 +339,9 @@
         ) * jnp.exp(hb)
         if b == 0:
             pl.semaphore_wait(barrier, groups - 1 + members - 1)
+            for t in range(3):
+                for side in range(2):
+                    shared_near(t, side).start()
             send_near(0)
 
     def decay_of(b, d):
@@ -372,6 +409,11 @@
         lax.fori_loop(1, groups, step, 0)
 
     each(lambda i: out_copy(peer_of(i), offset(i)).start())
+    for t in range(3):
+        for side in range(2):
+            shared_near(t, side).wait_recv()
+            shared_far(t, side).start()
+    send_cross(0)
     mine = pl.ds(pl.multiple_of(me * message, message), message)
     got_ref[mine, :] = send_ref[mine, :]
 
@@ -413,7 +455,9 @@
     lax.fori_loop(0, groups, scan, (zero, zero))
     each(lambda i: back_copy(peer_of(i), offset(i)).start())
     carry_ref[me] = back_state_ref[me]
-    send_far(0)
+    send_cross(1)
+    take_near(0)
+    send_far(0, (0,))
     each(lambda i: back_copy(peer_of(i), offset(i)).wait())
 
     state_f = jnp.concatenate([carry_ref[:, r, :] for r in range(share)], axis=0)
@@ -455,6 +499,11 @@
         mix_copy(i).start()
     send_near(1)
     send_near(2)
+    send_far(0, (1,))
+    for t in range(3):
+        for side in range(2):
+            shared_far(t, side).wait_recv()
+    send_cross(2)
     mixed_ref[row] = ks_ref[row]
 
     expert_id = lax.broadcasted_iota(jnp.int32, (LANES, count), 0)
@@ -542,51 +591,6 @@
         narrow(part)
         send_rows(arrived_ref, 0, part)
 
-    send_far(1)
-    send_near(3)
-    send_far(2)
-    for t in range(3):
-        for side in range(2):
-            shared_near(t, side).start()
-    for part in range(2):
-        take_rows(arrived_ref, 0, part)
-    for part in range(2):
-        get_lines(x_ref, part)
-    for copy in local_copies[1:]:
-        copy.wait()
-
-    def hide(slot):
-        g = jnp.dot(x_ref[...], gate_all[slot], preferred_element_type=F32)
-        u = jnp.dot(x_ref[...], up_all[slot], preferred_element_type=F32)
-        hidden_ref[:, slot * inner_width : (slot + 1) * inner_width] = (
-            g / (1.0 + jnp.exp(-g)) * u
-        ).astype(BF16)
-
-    for slot in range(3):
-        hide(slot)
-    send_far(3)
-    for t in range(2):
-        for side in range(2):
-            far_copy(t, side).wait_recv()
-    hide(3)
-    for part in range(2):
-        for side in range(2):
-            far_copy(2 + part, side).wait_recv()
-        for n in range(half_width // wide):
-            cols = pl.ds(part * half_width + n * wide, wide)
-            f = jnp.dot(hidden_ref[...], down_all[:, cols], preferred_element_type=F32)
-            put_lines(part, n * (wide // LANES), f)
-        narrow(part)
-        send_rows(back_ref, 2, part)
-
-    first_weight = jnp.where(first_named, weight_ref[0:1, :], 0.0)
-    weigh = first_weight + jnp.where(second_named, weight_ref[1:2, :], 0.0)
-    high = weigh.astype(BF16)
-    low = (weigh - high.astype(F32)).astype(BF16)
-    put = put_ref[...].astype(F32)
-    high = (jnp.dot(spread_ref[...], high, preferred_element_type=F32) * put).astype(BF16)
-    low = (jnp.dot(spread_ref[...], low, preferred_element_type=F32) * put).astype(BF16)
-
     def shared(gate, up, down, first):
         x = normed_ref[...]
         g = jnp.dot(x, gate[...], preferred_element_type=F32)
@@ -601,28 +605,75 @@
                 total_ref[:, cols] += more
 
     for t in range(3):
-        for side in range(2):
-            shared_near(t, side).wait_recv()
-            shared_far(t, side).start()
-            twin_copy(t, side, half_of(t, core)).start()
+        for k in range(3):
+            for n in range(1, stops):
+                cross_copy(t, k, n).wait_recv()
+            twin_copy(t, k, half_of(t, core)).start()
+    take_near(1)
+    send_far(1)
+    take_near(2)
+    send_far(2)
+    send_near(3)
     shared(sgate_ref, sup_ref, sdown_ref, True)
-    for t in range(3):
-        for side in range(2):
-            shared_far(t, side).wait_recv()
-        twin_copy(t, 2, half_of(t, core)).start()
     for k in range(3):
         for t in range(3):
             twin_copy(t, k, half_of(t, 1 - core)).wait_recv()
         shared(sgate_all.at[k], sup_all.at[k], sdown_all.at[k], False)
+    for part in range(2):
+        take_rows(arrived_ref, 0, part)
+    for part in range(2):
+        get_lines(x_ref, part)
+    for copy in local_copies[1:]:
+        copy.wait()
+
+    def hide(slot):
+        g = jnp.dot(x_ref[...], gate_all[slot], preferred_element_type=F32)
+        u = jnp.dot(x_ref[...], up_all[slot], preferred_element_type=F32)
+        hidden_ref[:, slot * inner_width : (slot + 1) * inner_width] = (
+            g / (1.0 + jnp.exp(-g)) * u
+        ).astype(BF16)
+
+    for slot in range(3):
+        hide(slot)
+    for t in range(2):
+        for side in range(2):
+            for sub in range(2):
+                far_copy(t, side, sub).wait_recv()
+    hide(3)
+    for part in range(2):
+        if part == 1:
+            take_near(3)
+            send_far(3)
+        for side in range(2):
+            for sub in range(2):
+                far_copy(2 + part, side, sub).wait_recv()
+        for n in range(half_width // wide):
+            cols = pl.ds(part * half_width + n * wide, wide)
+            f = jnp.dot(hidden_ref[...], down_all[:, cols], preferred_element_type=F32)
+            put_lines(part, n * (wide // LANES), f)
+        narrow(part)
+        send_rows(back_ref, 2, part)
+
+    first_weight = jnp.where(first_named, weight_ref[0:1, :], 0.0)
+    weigh = first_weight + jnp.where(second_named, weight_ref[1:2, :], 0.0)
+    high = weigh.astype(BF16)
+    low = (weigh - high.astype(F32)).astype(BF16)
+    put = put_ref[...].astype(F32)
+    high = (jnp.dot(spread_ref[...], high, preferred_element_type=F32) * put).astype(BF16)
+    low = (jnp.dot(spread_ref[...], low, preferred_element_type=F32) * put).astype(BF16)
+
     for t in range(4):
         for side in range(2):
             near_copy(t, side).wait_send()
-            far_copy(t, side).wait_send()
+            for sub in range(2):
+                far_copy(t, side, sub).wait_send()
     for t in range(3):
         for side in range(2):
             shared_near(t, side).wait_send()
             shared_far(t, side).wait_send()
         for k in range(3):
+            for n in range(1, stops):
+                cross_copy(t, k, n).wait_send()
             twin_copy(t, k, half_of(t, core)).wait_send()
 
     for part in range(2):
@@ -728,8 +779,10 @@
             dma((4, groups)),
             dma((14,)),
             dma((14,)),
-            dma((14,)),
-            dma((14,)),
+            dma((22,)),
+            dma((22,)),
+            dma((9 * min(4, groups // 2),)),
+            dma((9 * min(4, groups // 2),)),
             dma((9,)),
             dma((9,)),
             dma((4,)),

time: 170 us -> 159 us (0.935)
  Pallas kernels: 168 us -> 157 us
    pallas_call x1, Pallas kernels: 168 us -> 157 us  [body(): pl.pallas_call(functools.partial(layer_kernel, groups, members), out_shap...]
where the time goes in v4:
time: 159 us
  Pallas kernels  157 us (99%)
  local copies, waits for them, and re-layouts  1.88 us (1%)
    pallas_call x1, Pallas kernels, body(): pl.pallas_call(functools.partial(layer_kernel, groups, members), out_shap...  157 us

profile of v4, /device:TPU:1, one launch (start us, length us, event | category | flops | bytes accessed | tf_op | source)
XLA Modules:
  0.0 158.7 jit_solution(15271696519365571466)
XLA Ops:
  0.0 156.8 %layer.1 = bf16[128,2048]{1,0:T(8,128)(2,1)} custom-call(bf16[512,128]{1,0:T(8,128)(2,1)} %q_ref.1, bf16[512,128]{1,0:T(8,128)(2,1)} %k_ref.1, bf16[512,256]{1,0:T(8,128)(2,1)} %v_ref.1, bf16[512,256]{1,0:T(8,128)(2,1)} %g_ref.1, f32[512,128]{1,0:T(8,128)} %fd_ref.1, f32[512,128]{1,0:T(8,128)} %bd_ref.1, f32[1,256]{1,0:T(1,128)} %bitcast.15, ...), custom_call_target="tpu_custom_call" | custom-call | flops 10000000000 | bytes 100000000 | tf_op jit(solution)/shard_map/layer/pallas_call | solution.py:738
  156.8 1.9 %copy.26 = bf16[128,2048]{1,0:T(8,128)(2,1)} copy(bf16[128,2048]{1,0:T(8,128)(2,1)} %layer.1) | data formatting | bytes 1048576

commit v5 on v4

--- a/solution.py
+++ b/solution.py
@@ -13,6 +13,9 @@
 TOPK = 2
 CAP = 6
 CHUNK = 128
+OUT_PARTS = ((0, 16),)
+BACK_PARTS = ((0, 8), (8, 8))
+EARLY = 3
 LANES = 128
 EPS = 1e-06
 GATE_NORM = 16.0
@@ -120,9 +123,6 @@
     count, width = stream_ref.shape
     lines = width // LANES
     slots = put_ref.shape[0]
-    half_lines = lines // 2
-    half_rows = slots * half_lines
-    piece = half_rows // groups
     inner_width = gate_hbm.shape[1]
     sides = (lax.rem(row + 1, members), lax.rem(row + members - 1, members))
 
@@ -152,17 +152,21 @@
 
     half_width = width // 2
 
+    def columns_of(t):
+        first, number = BACK_PARTS[t - 2]
+        return pl.ds(first * LANES, number * LANES)
+
     def place(t, slot, start, size):
         if t < 2:
             whole = (gate_all, up_all)[t]
             return whole.at[slot, pl.ds(start, size)]
-        cols = pl.ds((t - 2) * half_width, half_width)
+        cols = columns_of(t)
         return down_all.at[pl.ds(slot * inner_width + start, size), cols]
 
     def shard(t):
         if t < 2:
             return (gate_hbm, up_hbm)[t]
-        return down_hbm.at[:, pl.ds((t - 2) * half_width, half_width)]
+        return down_hbm.at[:, columns_of(t)]
 
     def depth(t):
         return width if t < 2 else inner_width
@@ -222,8 +226,8 @@
         return pltpu.make_async_remote_copy(
             src_ref=shared_own[t].at[share_of(t)],
             dst_ref=shared_all[t].at[side, share_of(t)],
-            send_sem=near_send_sem.at[8 + 2 * t + side],
-            recv_sem=near_recv_sem.at[8 + 2 * t + side],
+            send_sem=near_send_sem.at[20 + 2 * t + side],
+            recv_sem=near_recv_sem.at[20 + 2 * t + side],
             device_id={"tp": sides[side]},
             device_id_type=MESH,
         )
@@ -239,8 +243,8 @@
         return pltpu.make_async_remote_copy(
             src_ref=part_of(t, side, side),
             dst_ref=part_of(t, 2, side),
-            send_sem=far_send_sem.at[16 + 2 * t + side],
-            recv_sem=far_recv_sem.at[16 + 2 * t + side],
+            send_sem=far_send_sem.at[40 + 2 * t + side],
+            recv_sem=far_recv_sem.at[40 + 2 * t + side],
             device_id={"tp": sides[side]},
             device_id_type=MESH,
         )
@@ -291,6 +295,12 @@
         return jnp.dot(tri, high, preferred_element_type=F32) + jnp.dot(
             tri, low, preferred_element_type=F32
         )
+
+    pl.semaphore_wait(barrier, groups - 1 + members - 1)
+    for t in range(3):
+        for side in range(2):
+            shared_near(t, side).start()
+    send_near(0)
 
     for b in range(chunks):
         rows = slice(b * CHUNK, (b + 1) * CHUNK)
@@ -337,12 +347,6 @@
         upd_ref[2 * b + 1] = jnp.where(
             first_head, both[0:DV, LANES : 2 * LANES], both[DV : 2 * DV, LANES : 2 * LANES]
         ) * jnp.exp(hb)
-        if b == 0:
-            pl.semaphore_wait(barrier, groups - 1 + members - 1)
-            for t in range(3):
-                for side in range(2):
-                    shared_near(t, side).start()
-            send_near(0)
 
     def decay_of(b, d):
         return jnp.exp(half_ref[2 * b + d : 2 * b + d + 1, :] * 2.0)
@@ -497,8 +501,8 @@
             ks_ref[b, :, cols] = o.astype(BF16)
     for i in range(1, members):
         mix_copy(i).start()
-    send_near(1)
-    send_near(2)
+    for t in range(1, EARLY):
+        send_near(t)
     send_far(0, (1,))
     for t in range(3):
         for side in range(2):
@@ -537,25 +541,30 @@
         normed_ref[rows, :] = r.astype(BF16)
 
     def piece_of(part, i):
-        return pl.ds(pl.multiple_of(part * half_rows + i * piece, 16), piece)
-
-    def row_copy(src, dst, base, part, i):
+        first, number = part
+        piece = slots * number // groups
+        return pl.ds(pl.multiple_of(slots * first + i * piece, 8), piece)
+
+    def row_copy(src, dst, sem, part, i):
         peer = peer_of(i)
         return pltpu.make_async_remote_copy(
             src_ref=src.at[piece_of(part, peer)],
             dst_ref=dst.at[piece_of(part, me)],
-            send_sem=row_send_sem.at[base + part, offset(i)],
-            recv_sem=row_recv_sem.at[base + part, offset(i)],
+            send_sem=row_send_sem.at[sem, offset(i)],
+            recv_sem=row_recv_sem.at[sem, offset(i)],
             device_id={"sp": peer},
             device_id_type=MESH,
         )
 
-    def put_lines(part, line, array):
-        for k in range(array.shape[1] // LANES):
-            at = pl.ds(part * half_rows + line + k, slots, stride=half_lines)
-            stage_ref[at, :] = array[:, k * LANES : (k + 1) * LANES]
-
-    def narrow(part):
+    def fill_rows(part, left, right):
+        first, number = part
+        for n in range(number // 2):
+            cols = pl.ds((first + 2 * n) * LANES, 2 * LANES)
+            f = jnp.dot(left[...], right[:, cols], preferred_element_type=F32)
+            for k in range(2):
+                at = pl.ds(slots * first + 2 * n + k, slots, stride=number)
+                stage_ref[at, :] = f[:, k * LANES : (k + 1) * LANES]
+
         def one(i, c):
             filled_ref[piece_of(part, i), :] = stage_ref[piece_of(part, i), :].astype(BF16)
             return c
@@ -563,33 +572,29 @@
         lax.fori_loop(0, groups, one, 0)
 
     def get_lines(dst, part):
-        for k in range(half_lines):
-            at = pl.ds(part * half_rows + k, slots, stride=half_lines)
-            n = part * half_lines + k
+        first, number = part
+        for k in range(number):
+            at = pl.ds(slots * first + k, slots, stride=number)
+            n = first + k
             dst[:, n * LANES : (n + 1) * LANES] = stage_ref[at, :].astype(BF16)
 
-    def send_rows(dst, base, part):
-        each(lambda i: row_copy(filled_ref, dst, base, part, i).start())
-
-    def take_rows(dst, base, part):
+    def send_rows(dst, sem, part):
+        each(lambda i: row_copy(filled_ref, dst, sem, part, i).start())
+
+    def take_rows(dst, sem, part):
         own = piece_of(part, me)
         stage_ref[own, :] = filled_ref[own, :].astype(F32)
 
         def one(i):
-            row_copy(filled_ref, dst, base, part, i).wait()
+            row_copy(filled_ref, dst, sem, part, i).wait()
             came = piece_of(part, lax.rem(me + groups - offset(i), groups))
             stage_ref[came, :] = dst[came, :].astype(F32)
 
         each(one)
 
-    wide = min(2 * LANES, half_width)
-    for part in range(2):
-        for n in range(half_width // wide):
-            cols = pl.ds(part * half_width + n * wide, wide)
-            f = jnp.dot(put_ref[...], normed_ref[:, cols], preferred_element_type=F32)
-            put_lines(part, n * (wide // LANES), f)
-        narrow(part)
-        send_rows(arrived_ref, 0, part)
+    for sem, part in enumerate(OUT_PARTS):
+        fill_rows(part, put_ref, normed_ref)
+        send_rows(arrived_ref, sem, part)
 
     def shared(gate, up, down, first):
         x = normed_ref[...]
@@ -613,15 +618,19 @@
     send_far(1)
     take_near(2)
     send_far(2)
-    send_near(3)
+    for t in range(EARLY, 2 + len(BACK_PARTS)):
+        send_near(t)
+    for t in range(3, EARLY):
+        take_near(t)
+        send_far(t)
     shared(sgate_ref, sup_ref, sdown_ref, True)
     for k in range(3):
         for t in range(3):
             twin_copy(t, k, half_of(t, 1 - core)).wait_recv()
         shared(sgate_all.at[k], sup_all.at[k], sdown_all.at[k], False)
-    for part in range(2):
-        take_rows(arrived_ref, 0, part)
-    for part in range(2):
+    for sem, part in enumerate(OUT_PARTS):
+        take_rows(arrived_ref, sem, part)
+    for part in OUT_PARTS:
         get_lines(x_ref, part)
     for copy in local_copies[1:]:
         copy.wait()
@@ -640,19 +649,16 @@
             for sub in range(2):
                 far_copy(t, side, sub).wait_recv()
     hide(3)
-    for part in range(2):
-        if part == 1:
-            take_near(3)
-            send_far(3)
+    sent = EARLY
+    for n, part in enumerate(BACK_PARTS):
+        if 2 + n >= sent:
+            take_near(2 + n)
+            send_far(2 + n)
         for side in range(2):
             for sub in range(2):
-                far_copy(2 + part, side, sub).wait_recv()
-        for n in range(half_width // wide):
-            cols = pl.ds(part * half_width + n * wide, wide)
-            f = jnp.dot(hidden_ref[...], down_all[:, cols], preferred_element_type=F32)
-            put_lines(part, n * (wide // LANES), f)
-        narrow(part)
-        send_rows(back_ref, 2, part)
+                far_copy(2 + n, side, sub).wait_recv()
+        fill_rows(part, hidden_ref, down_all)
+        send_rows(back_ref, len(OUT_PARTS) + n, part)
 
     first_weight = jnp.where(first_named, weight_ref[0:1, :], 0.0)
     weigh = first_weight + jnp.where(second_named, weight_ref[1:2, :], 0.0)
@@ -662,7 +668,7 @@
     high = (jnp.dot(spread_ref[...], high, preferred_element_type=F32) * put).astype(BF16)
     low = (jnp.dot(spread_ref[...], low, preferred_element_type=F32) * put).astype(BF16)
 
-    for t in range(4):
+    for t in range(2 + len(BACK_PARTS)):
         for side in range(2):
             near_copy(t, side).wait_send()
             for sub in range(2):
@@ -676,11 +682,11 @@
                 cross_copy(t, k, n).wait_send()
             twin_copy(t, k, half_of(t, core)).wait_send()
 
-    for part in range(2):
-        take_rows(back_ref, 2, part)
+    for n, part in enumerate(BACK_PARTS):
+        take_rows(back_ref, len(OUT_PARTS) + n, part)
         get_lines(x_ref, part)
-        for n in range(half_width // wide):
-            cols = pl.ds(part * half_width + n * wide, wide)
+        for k in range(part[1] // 2):
+            cols = pl.ds((part[0] + 2 * k) * LANES, 2 * LANES)
             total_ref[:, cols] += lax.dot_general(
                 high, x_ref[:, cols], TN, preferred_element_type=F32
             ) + lax.dot_general(low, x_ref[:, cols], TN, preferred_element_type=F32)
@@ -775,12 +781,12 @@
             dma((groups,)),
             dma((members,)),
             dma((members,)),
-            dma((4, groups)),
-            dma((4, groups)),
-            dma((14,)),
-            dma((14,)),
-            dma((22,)),
-            dma((22,)),
+            dma((len(OUT_PARTS) + len(BACK_PARTS), groups)),
+            dma((len(OUT_PARTS) + len(BACK_PARTS), groups)),
+            dma((26,)),
+            dma((26,)),
+            dma((46,)),
+            dma((46,)),
             dma((9 * min(4, groups // 2),)),
             dma((9 * min(4, groups // 2),)),
             dma((9,)),

time: 159 us -> 158 us (level)
  no operation moved by 1% of the time
where the time goes in v5:
time: 158 us
  Pallas kernels  156 us (99%)
  local copies, waits for them, and re-layouts  1.88 us (1%)
    pallas_call x1, Pallas kernels, body(): pl.pallas_call(functools.partial(layer_kernel, groups, members), out_shap...  156 us

profile of v5, /device:TPU:1, one launch (start us, length us, event | category | flops | bytes accessed | tf_op | source)
XLA Modules:
  0.0 158.0 jit_solution(452667276294372387)
XLA Ops:
  0.0 156.1 %layer.1 = bf16[128,2048]{1,0:T(8,128)(2,1)} custom-call(bf16[512,128]{1,0:T(8,128)(2,1)} %q_ref.1, bf16[512,128]{1,0:T(8,128)(2,1)} %k_ref.1, bf16[512,256]{1,0:T(8,128)(2,1)} %v_ref.1, bf16[512,256]{1,0:T(8,128)(2,1)} %g_ref.1, f32[512,128]{1,0:T(8,128)} %fd_ref.1, f32[512,128]{1,0:T(8,128)} %bd_ref.1, f32[1,256]{1,0:T(1,128)} %bitcast.15, ...), custom_call_target="tpu_custom_call" | custom-call | flops 10000000000 | bytes 100000000 | tf_op jit(solution)/shard_map/layer/pallas_call | solution.py:744
  156.2 1.9 %copy.26 = bf16[128,2048]{1,0:T(8,128)(2,1)} copy(bf16[128,2048]{1,0:T(8,128)(2,1)} %layer.1) | data formatting | bytes 1048576
